TPU v7x, 256 devices: a whole 4x4x8 slice. The times are simulated.
256 devices in a mesh: kv: 32 (over z, x), tp: 8 (over y, core).
Axes of the slice: x: 4, y: 4, z: 8, core: 2. Of those that a mesh axis runs over, the one named last changes fastest.
Arguments:
- tokens: bfloat16 [18, 4096], P(None, ('kv', 'tp')), may hold values from -12.2 to 12.2
- norm_gains: float32 [6, 4096], replicated, may hold values from 0.1 to 1.9
- first_gate: bfloat16 [4096, 11264], P(None, ('kv', 'tp')), may hold values from -0.09375 to 0.09375
- first_lift: bfloat16 [4096, 11264], P(None, ('kv', 'tp')), may hold values from -0.09375 to 0.09375
- first_down: bfloat16 [11264, 4096], P(('kv', 'tp')), may hold values from -0.25 to 0.25
- query_weight: bfloat16 [4096, 4096], P('kv', 'tp'), may hold values from -0.09375 to 0.09375
- key_weight: bfloat16 [4096, 4096], P('kv', 'tp'), may hold values from -0.09375 to 0.09375
- value_weight: bfloat16 [4096, 4096], P('kv', 'tp'), may hold values from -0.09375 to 0.09375
- forget_weight: bfloat16 [4096, 64], P(None, 'tp'), may hold values from -0.25 to 0.25
- output_weight: bfloat16 [4096, 4096], P('tp', 'kv'), may hold values from -0.09375 to 0.09375
- second_gate: bfloat16 [4096, 11264], P(None, ('kv', 'tp')), may hold values from -0.09375 to 0.09375
- second_lift: bfloat16 [4096, 11264], P(None, ('kv', 'tp')), may hold values from -0.09375 to 0.09375
- second_down: bfloat16 [11264, 4096], P(('kv', 'tp')), may hold values from -0.25 to 0.25
- cache_keys: bfloat16 [18, 8192, 4096], P(None, 'kv', 'tp'), may hold values from -457 to 457
- cache_values: bfloat16 [18, 8192, 4096], P(None, 'kv', 'tp'), may hold values from -6 to 6
- cache_decay: float32 [18, 64, 8192], P(None, 'tp', 'kv'), may hold values from -2500 to 0, as said below
Outputs:
- layer_out: bfloat16 [18, 4096], P(None, ('kv', 'tp'))
Inputs may be any that keep to these rules, and one draw needn't show every extreme that they name: `cache_decay`: each entry is a sum of log forget gates, each at most zero, of the later cached positions of the same sequence and head, so entries never fall along positions and the last is zero.
All inputs are finite; a program needn't handle non-finite values.
Results may differ from a plain program's by a relative error of at most 0.025.
Values may be sent and summed in bfloat16 or wider, within the bound.
A program may use at most 64 MiB of HBM per device.

v0:
```python
import jax
import jax.numpy as jnp
from jax import lax
from jax.sharding import Mesh
from jax.sharding import PartitionSpec as P

HD = 64
KV_TP = ("kv_0", "kv_1", "tp_0", "tp_1")
KV = ("kv_0", "kv_1")
TP = ("tp_0", "tp_1")


epsilon = 1e-06


def cut_along(value, dim, count):
    lengths = value.shape
    tiles = value.reshape(*lengths[:dim], count, lengths[dim] // count, *lengths[dim + 1 :])
    return jnp.moveaxis(tiles, dim, 0)


def sum_at_owner(value, axis, dim):
    tiles = cut_along(value, dim, lax.axis_size(axis))
    arrived = lax.all_to_all(tiles, axis, split_axis=0, concat_axis=0, tiled=True)
    return arrived.sum(axis=0)


def summed_rows(value, axes, dim):
    far, near = axes
    tiles = cut_along(value, dim, lax.axis_size(far))
    nearer = sum_at_owner(tiles, near, dim + 1)
    arrived = lax.all_to_all(nearer, far, split_axis=0, concat_axis=0, tiled=True)
    return arrived.sum(axis=0)


def rows_for(lines, count):
    spare = -lines.shape[0] % count
    if not spare:
        return lines
    return jnp.concatenate([lines, jnp.zeros((spare, *lines.shape[1:]), lines.dtype)])


def sent_to_all(value, axis):
    count = lax.axis_size(axis)
    return lax.all_to_all(
        jnp.broadcast_to(value[None], (count, *value.shape)), axis, 0, 0, tiled=True
    )


def in_order(tiles, dim):
    tiles = jnp.moveaxis(tiles, 0, dim)
    lengths = tiles.shape
    return tiles.reshape(*lengths[:dim], lengths[dim] * lengths[dim + 1], *lengths[dim + 2 :])


def gathered_by_axis(value, axes, dim):
    far, near = axes
    tiles = sent_to_all(sent_to_all(value, far), near)
    return in_order(tiles.swapaxes(0, 1).reshape(-1, *value.shape), dim)


def sum_by_parts(value, axes):
    lines = value.reshape(-1)
    own = summed_rows(rows_for(lines, lax.axis_size(axes[0]) * lax.axis_size(axes[1])), axes, 0)
    whole = gathered_by_axis(own, axes, 0)
    return whole[: len(lines)].reshape(value.shape)


def collect(value, axis, dim):
    tiles = sent_to_all(value, axis)
    return in_order(tiles, dim)


def sent_and_summed(value, axis, dim):
    count = lax.axis_size(axis)
    tiles = lax.all_to_all(cut_along(value, dim, count), axis, 0, 0, tiled=True)
    return jnp.sum(tiles.astype(jnp.float32), axis=0)


def sum_by_parts_2(value, axes):
    lines = value.reshape(-1)
    padded = rows_for(lines, lax.axis_size(axes))
    whole = collect(sent_and_summed(padded, axes, 0).astype(jnp.bfloat16), axes, 0)
    return lax.slice_in_dim(whole, 0, len(lines)).reshape(value.shape).astype(jnp.float32)


def all_in_one(value, axis):
    leaves = jax.tree.leaves(value)
    sequence = sorted(range(len(leaves)), key=lambda k: -leaves[k].size)
    width = (1, *leaves[sequence[0]].shape)[-1]
    lines = [
        jnp.pad(leaves[k].reshape(-1), (0, -leaves[k].size % width)).reshape(-1, width)
        for k in sequence
    ]
    both, at, found = (lax.all_gather(jnp.concatenate(lines), axis), 0, {})
    for k, line in zip(sequence, lines):
        piece = both[:, at : at + len(line)].reshape(len(both), -1)
        found[k] = piece[:, : leaves[k].size].reshape(-1, *leaves[k].shape)
        at += len(line)
    numbers = iter(range(len(leaves)))
    return jax.tree.map(lambda _: found[next(numbers)], value)


def combined_by_axis(value, axes, combine):
    for axis in axes:
        pieces = all_in_one(
            jax.tree.map(
                lambda part, kind: part.astype(kind),
                value,
                (jnp.bfloat16, jnp.bfloat16, jnp.bfloat16),
            ),
            axis,
        )
        widened = [
            jax.tree.map(lambda part, own: part[k].astype(own.dtype), pieces, value)
            for k in range(lax.axis_size(axis))
        ]
        value = widened[0]
        for received in widened[1:]:
            value = combine(value, received)
    return value


def of_everyone(value, axis):
    everything = sent_to_all(value, axis)
    return jnp.sum(everything.astype(jnp.float32), axis=0)


def root_norm(values, norm_gain):
    return (
        values * lax.rsqrt(jnp.mean(values * values, axis=-1, keepdims=True) + epsilon) * norm_gain
    )


def settle(values):
    return lax.optimization_barrier(values.astype(jnp.bfloat16)).astype(jnp.float32)


def gated_terms(stream, pre_gain, gate_matrix, lift_matrix, down_matrix):
    normed = root_norm(stream, pre_gain).astype(jnp.bfloat16)
    gate_part = jnp.dot(normed, gate_matrix, preferred_element_type=jnp.float32)
    lift_part = jnp.dot(normed, lift_matrix, preferred_element_type=jnp.float32)
    active = (jax.nn.silu(gate_part) * lift_part).astype(jnp.bfloat16)
    return jnp.dot(active, down_matrix, preferred_element_type=jnp.float32)


def branch_total(partial_value):
    summed = sum_by_parts(partial_value, (("kv_0", "kv_1"), ("tp_0", "tp_1")))
    return summed


def spread_heads(per_head):
    return jnp.repeat(per_head, HD, axis=-1)


def join_pair(first, second):
    peak_first, total_first, out_first = first
    peak_second, total_second, out_second = second
    summit = jnp.maximum(peak_first, peak_second)
    weight_first = total_first * jnp.exp(peak_first - summit)
    weight_second = total_second * jnp.exp(peak_second - summit)
    joined = spread_heads(weight_first) * out_first + spread_heads(weight_second) * out_second
    joined = joined / spread_heads(weight_first + weight_second)
    return (summit, weight_first + weight_second, joined)


def body(
    tokens,
    norm_gains,
    first_gate,
    first_lift,
    first_down,
    query_weight,
    key_weight,
    value_weight,
    forget_weight,
    output_weight,
    second_gate,
    second_lift,
    second_down,
    cache_keys,
    cache_values,
    cache_decay,
):
    seq_count = tokens.shape[0]
    own_width = tokens.shape[1]
    own_start = lax.axis_index(KV_TP) * own_width
    stream = gathered_by_axis(tokens, (("kv_0", "kv_1"), ("tp_0", "tp_1")), 1).astype(jnp.float32)
    first_sum = branch_total(gated_terms(stream, norm_gains[0], first_gate, first_lift, first_down))
    first_branch = settle(first_sum)
    middle = stream + 0.5 * root_norm(first_branch, norm_gains[1])
    normed = root_norm(middle, norm_gains[2]).astype(jnp.bfloat16)
    block_rows = query_weight.shape[0]
    feature_block = lax.dynamic_slice_in_dim(normed, lax.axis_index(KV) * block_rows, block_rows, 1)
    query_part = jnp.dot(feature_block, query_weight, preferred_element_type=jnp.float32)
    key_part = jnp.dot(feature_block, key_weight, preferred_element_type=jnp.float32)
    value_part = jnp.dot(feature_block, value_weight, preferred_element_type=jnp.float32)
    queries, key_new, value_new = (
        sum_by_parts_2(query_part.astype(jnp.bfloat16), KV),
        sum_by_parts_2(key_part.astype(jnp.bfloat16), KV),
        sum_by_parts_2(value_part.astype(jnp.bfloat16), KV),
    )
    queries = queries.astype(jnp.bfloat16)
    key_new = key_new.astype(jnp.bfloat16)
    value_new = value_new.astype(jnp.bfloat16)
    forget = jax.nn.log_sigmoid(jnp.dot(normed, forget_weight, preferred_element_type=jnp.float32))
    head_count = forget_weight.shape[1]
    position_index = cache_keys.shape[1]
    score_scale = HD ** (-0.5)
    query_heads = queries.reshape(seq_count, head_count, HD)
    key_heads = cache_keys.reshape(seq_count, position_index, head_count, HD)
    value_heads = cache_values.reshape(seq_count, position_index, head_count, HD)
    scores = (
        jnp.einsum("bhd,bphd->bhp", query_heads, key_heads, preferred_element_type=jnp.float32)
        * score_scale
    )
    scores = scores + forget[:, :, None] + cache_decay
    block_peak = jnp.max(scores, axis=2)
    raised = jnp.exp(scores - block_peak[:, :, None])
    block_total = jnp.sum(raised, axis=2)
    weighted = jnp.einsum(
        "bhp,bphd->bhd",
        raised.astype(jnp.bfloat16),
        value_heads,
        preferred_element_type=jnp.float32,
    )
    block_out = settle(weighted / block_total[:, :, None]).reshape(seq_count, head_count * HD)
    own_score = (
        jnp.einsum(
            "bhd,bhd->bh",
            query_heads,
            key_new.reshape(seq_count, head_count, HD),
            preferred_element_type=jnp.float32,
        )
        * score_scale
    )
    own_part = (own_score, jnp.ones_like(own_score), value_new.astype(jnp.float32))
    merged = combined_by_axis((block_peak, block_total, block_out), KV, join_pair)
    summit, weight_sum, joined = join_pair(merged, own_part)
    attended = joined.astype(jnp.bfloat16)
    projected = settle(jnp.dot(attended, output_weight, preferred_element_type=jnp.float32))
    mixed_block = (
        of_everyone(projected.astype(jnp.bfloat16), TP).astype(jnp.float32).astype(jnp.bfloat16)
    )
    mixed_rows = collect(mixed_block, KV, 1).astype(jnp.float32)
    after_mix = middle + root_norm(mixed_rows, norm_gains[3])
    second_sum = branch_total(
        gated_terms(after_mix, norm_gains[4], second_gate, second_lift, second_down)
    )
    own_rows = lax.dynamic_slice_in_dim(after_mix, own_start, own_width, 1)
    second_branch = lax.dynamic_slice_in_dim(
        root_norm(settle(second_sum), norm_gains[5]), own_start, own_width, 1
    )
    return (own_rows + 0.5 * second_branch).astype(jnp.bfloat16)


def solution(mesh):
    finer = Mesh(mesh.devices.reshape(8, 4, 4, 2), ("kv_0", "kv_1", "tp_0", "tp_1"))
    placed = (
        P(None, KV_TP),
        P(),
        P(None, KV_TP),
        P(None, KV_TP),
        P(KV_TP, None),
        P(KV, TP),
        P(KV, TP),
        P(KV, TP),
        P(None, TP),
        P(TP, KV),
        P(None, KV_TP),
        P(None, KV_TP),
        P(KV_TP, None),
        P(None, KV, TP),
        P(None, KV, TP),
        P(None, TP, KV),
    )
    return jax.shard_map(
        body, mesh=finer, in_specs=placed, out_specs=P(None, KV_TP), check_vma=False
    )
```

profile of v0, /device:TPU:1, one launch (start us, length us, event | category | flops | bytes accessed | tf_op | source)
XLA Modules:
  0.0 314.6 jit_solution(12728453481438157856)
XLA Ops:
  0.0 0.8 broadcast_bitcast_fusion.1
  0.9 20.4 %all_to_all.118 = bf16[32,2,144]{2,1,0:T(2,128)(2,1)S(1)} all-to-all(bf16[32,2,144]{2,1,0:T(2,128)(2,1)S(1)} %reshape.694), channel_id=1, replica_groups=mesh['kv_0'=8,'kv_1'=4,'tp_0'=4,'tp_1'=2] {'kv_0','kv_1'}, dimensions={0} | all-to-all | bytes 36864 | tf_op jit(solution)/shard_map/all_to_all | solution.py:45
  21.7 1.1 reshape.696
  22.8 6.6 %all-to-all-start.1 = ((bf16[8,2,4608]{2,1,0:T(2,128)(2,1)}), bf16[8,2,4608]{2,1,0:T(2,128)(2,1)S(1)}, u32[]{:S(2)}, u32[]{:S(2)}) async-start(bf16[8,2,4608]{2,1,0:T(2,128)(2,1)} %reshape.696), calls=%async_computation.1 | async-start | bytes 294912 | tf_op jit(solution)/shard_map/all_to_all | solution.py:45
  29.4 1.4 fusion.119
  30.8 4.0 %all-to-all-done.1 = bf16[8,2,4608]{2,1,0:T(2,128)(2,1)S(1)} async-done(((bf16[8,2,4608]{2,1,0:T(2,128)(2,1)}), bf16[8,2,4608]{2,1,0:T(2,128)(2,1)S(1)}, u32[]{:S(2)}, u32[]{:S(2)}) %all-to-all-start.1) | async-done | bytes 147488 | tf_op jit(solution)/shard_map/all_to_all | solution.py:45
  34.8 0.3 reshape.697
  35.4 1.1 convert_bitcast_fusion
  36.5 2.0 copy.109
  38.5 1.7 reshape.496
  40.2 1.3 fusion.108
  41.5 1.6 fusion.4
  43.1 0.3 reshape_reshape_reshape.8
  43.5 11.3 %all_to_all.119 = f32[8,32,288]{2,1,0:T(8,128)S(1)} all-to-all(f32[8,32,288]{2,1,0:T(8,128)S(1)} %bitcast.169), channel_id=1, replica_groups=mesh['kv_0'=8,'kv_1'=4,'tp_0'=4,'tp_1'=2] {'tp_0','tp_1'}, dimensions={0} | all-to-all | bytes 589824 | tf_op jit(solution)/shard_map/all_to_all | solution.py:24
  54.9 11.7 %all_to_all.120 = f32[32,1,288]{2,1,0:T(1,128)S(1)} all-to-all(f32[32,1,288]{2,1,0:T(1,128)S(1)} %all_to_all.77), channel_id=1, replica_groups=mesh['kv_0'=8,'kv_1'=4,'tp_0'=4,'tp_1'=2] {'kv_0','kv_1'}, dimensions={0} | all-to-all | bytes 73728 | tf_op jit(solution)/shard_map/all_to_all | solution.py:32
  66.7 0.5 broadcast.195
  67.2 0.8 reduce.118
  68.1 11.7 %all_to_all.121 = bf16[32,2,144]{2,1,0:T(2,128)(2,1)S(1)} all-to-all(bf16[32,2,144]{2,1,0:T(2,128)(2,1)S(1)} %reshape.698), channel_id=1, replica_groups=mesh['kv_0'=8,'kv_1'=4,'tp_0'=4,'tp_1'=2] {'kv_0','kv_1'}, dimensions={0} | all-to-all | bytes 36864 | tf_op jit(solution)/shard_map/all_to_all | solution.py:45
  79.9 0.7 broadcast_in_dim.182
  80.6 6.4 %all-to-all-start.5 = ((bf16[8,32,288]{2,1,0:T(8,128)(2,1)}), bf16[8,32,288]{2,1,0:T(8,128)(2,1)S(1)}, u32[]{:S(2)}, u32[]{:S(2)}) async-start(bf16[8,32,288]{2,1,0:T(8,128)(2,1)} %broadcast_in_dim.182), calls=%async_computation.5 | async-start | bytes 393216 | tf_op jit(solution)/shard_map/all_to_all | solution.py:45
  87.0 5.9 %all-to-all-done.5 = bf16[8,32,288]{2,1,0:T(8,128)(2,1)S(1)} async-done(((bf16[8,32,288]{2,1,0:T(8,128)(2,1)}), bf16[8,32,288]{2,1,0:T(8,128)(2,1)S(1)}, u32[]{:S(2)}, u32[]{:S(2)}) %all-to-all-start.5) | async-done | bytes 147488 | tf_op jit(solution)/shard_map/all_to_all | solution.py:45
  93.0 0.3 convert_element_type.484
  94.2 0.8 reduce.121
  95.0 0.7 reshape.704
  95.7 3.8 %all-to-all-start.8 = ((bf16[32,2,144]{2,1,0:T(2,128)(2,1)}), bf16[32,2,144]{2,1,0:T(2,128)(2,1)S(1)}, u32[]{:S(2)}, u32[]{:S(2)}) async-start(bf16[32,2,144]{2,1,0:T(2,128)(2,1)} %reshape.704), calls=%async_computation.8 | async-start | bytes 65536 | tf_op jit(solution)/shard_map/all_to_all | solution.py:76
  99.8 0.8 reduce.119
  100.6 0.7 reshape.700
  101.3 6.9 %all-to-all-done.8 = bf16[32,2,144]{2,1,0:T(2,128)(2,1)S(1)} async-done(((bf16[32,2,144]{2,1,0:T(2,128)(2,1)}), bf16[32,2,144]{2,1,0:T(2,128)(2,1)S(1)}, u32[]{:S(2)}, u32[]{:S(2)}) %all-to-all-start.8) | async-done | bytes 18464 | tf_op jit(solution)/shard_map/all_to_all | solution.py:76
  108.2 3.9 %all-to-all-start.6 = ((bf16[32,2,144]{2,1,0:T(2,128)(2,1)}), bf16[32,2,144]{2,1,0:T(2,128)(2,1)S(1)}, u32[]{:S(2)}, u32[]{:S(2)}) async-start(bf16[32,2,144]{2,1,0:T(2,128)(2,1)} %reshape.700), calls=%async_computation.6 | async-start | bytes 65536 | tf_op jit(solution)/shard_map/all_to_all | solution.py:76
  112.3 0.8 reduce.123
  113.1 0.7 reshape.708
  113.8 6.9 %all-to-all-done.6 = bf16[32,2,144]{2,1,0:T(2,128)(2,1)S(1)} async-done(((bf16[32,2,144]{2,1,0:T(2,128)(2,1)}), bf16[32,2,144]{2,1,0:T(2,128)(2,1)S(1)}, u32[]{:S(2)}, u32[]{:S(2)}) %all-to-all-start.6) | async-done | bytes 18464 | tf_op jit(solution)/shard_map/all_to_all | solution.py:76
  120.7 3.9 %all-to-all-start.10 = ((bf16[32,2,144]{2,1,0:T(2,128)(2,1)}), bf16[32,2,144]{2,1,0:T(2,128)(2,1)S(1)}, u32[]{:S(2)}, u32[]{:S(2)}) async-start(bf16[32,2,144]{2,1,0:T(2,128)(2,1)} %reshape.708), calls=%async_computation.10 | async-start | bytes 65536 | tf_op jit(solution)/shard_map/all_to_all | solution.py:76
  124.6 6.6 %copy.90 = bf16[18,256,512]{1,2,0:T(8,128)(2,1)} copy(bf16[18,256,512]{2,1,0:T(8,128)(2,1)} %param.29) | data formatting | bytes 9437184 | tf_op args[13]
  131.2 6.7 %copy.92 = bf16[18,256,512]{1,2,0:T(8,128)(2,1)} copy(bf16[18,256,512]{2,1,0:T(8,128)(2,1)} %param.30) | data formatting | bytes 9437184 | tf_op args[14]
  138.1 0.8 reduce.120
  138.9 0.7 reshape.702
  139.6 9.4 %all-to-all-start.7 = ((bf16[32,2,144]{2,1,0:T(2,128)(2,1)}), bf16[32,2,144]{2,1,0:T(2,128)(2,1)S(1)}, u32[]{:S(2)}, u32[]{:S(2)}) async-start(bf16[32,2,144]{2,1,0:T(2,128)(2,1)} %reshape.702), calls=%async_computation.7 | async-start | bytes 65536 | tf_op jit(solution)/shard_map/all_to_all | solution.py:45
  149.7 0.8 reduce.124
  150.5 0.7 reshape.710
  151.2 0.8 reduce.122
  152.0 0.7 reshape.706
  152.7 4.8 %all-to-all-done.7 = bf16[32,2,144]{2,1,0:T(2,128)(2,1)S(1)} async-done(((bf16[32,2,144]{2,1,0:T(2,128)(2,1)}), bf16[32,2,144]{2,1,0:T(2,128)(2,1)S(1)}, u32[]{:S(2)}, u32[]{:S(2)}) %all-to-all-start.7) | async-done | bytes 18464 | tf_op jit(solution)/shard_map/all_to_all | solution.py:45
  157.4 4.3 %all-to-all-start.11 = ((bf16[32,2,144]{2,1,0:T(2,128)(2,1)}), bf16[32,2,144]{2,1,0:T(2,128)(2,1)S(1)}, u32[]{:S(2)}, u32[]{:S(2)}) async-start(bf16[32,2,144]{2,1,0:T(2,128)(2,1)} %reshape.710), calls=%async_computation.11 | async-start | bytes 65536 | tf_op jit(solution)/shard_map/all_to_all | solution.py:45
  162.1 3.1 fusion.121
  165.8 3.6 %fusion.12 = f32[18,8,1,64]{3,2,1,0:T(1,128)S(1)} fusion(bf16[18,256,8,64]{1,3,2,0:T(8,128)(2,1)} %bitcast.168, bf16[18,8,256,1]{2,1,0,3:T(8,128)(2,1)S(1)} %get-tuple-element.71), kind=kOutput, calls=%fused_computation.37 | convolution fusion | flops 4718592 | bytes 4829184 | tf_op jit(solution)/shard_map/bhp,bphd->bhd/dot_general | solution.py:221
  169.7 20.0 %all-gather.2 = bf16[8,20,512]{2,1,0:T(8,128)(2,1)S(1)} all-gather(bf16[1,20,512]{2,1,0:T(8,128)(2,1)S(1)} %maximum_bitcast_fusion), channel_id=2, replica_groups=mesh['kv_0'=8,'kv_1'=4,'tp_0'=4,'tp_1'=2] {'kv_0'}, dimensions={0}, use_global_device_ids=true | all-gather | bytes 184320 | tf_op jit(solution)/shard_map/all_gather | solution.py:95
  189.8 7.9 %all-to-all-start.9 = ((bf16[32,2,144]{2,1,0:T(2,128)(2,1)}), bf16[32,2,144]{2,1,0:T(2,128)(2,1)S(1)}, u32[]{:S(2)}, u32[]{:S(2)}) async-start(bf16[32,2,144]{2,1,0:T(2,128)(2,1)} %reshape.706), calls=%async_computation.9 | async-start | bytes 65536 | tf_op jit(solution)/shard_map/all_to_all | solution.py:45
  198.2 8.2 %all-to-all-done.9 = bf16[32,2,144]{2,1,0:T(2,128)(2,1)S(1)} async-done(((bf16[32,2,144]{2,1,0:T(2,128)(2,1)}), bf16[32,2,144]{2,1,0:T(2,128)(2,1)S(1)}, u32[]{:S(2)}, u32[]{:S(2)}) %all-to-all-start.9) | async-done | bytes 18464 | tf_op jit(solution)/shard_map/all_to_all | solution.py:45
  212.1 9.5 %all-gather.3 = bf16[4,20,512]{2,1,0:T(8,128)(2,1)S(1)} all-gather(bf16[1,20,512]{2,1,0:T(8,128)(2,1)S(1)} %maximum_bitcast_fusion.1), channel_id=3, replica_groups=mesh['kv_0'=8,'kv_1'=4,'tp_0'=4,'tp_1'=2] {'kv_1'}, dimensions={0}, use_global_device_ids=true | all-gather | bytes 102400 | tf_op jit(solution)/shard_map/all_gather | solution.py:95
  224.8 22.1 %all_to_all.122 = bf16[8,18,128]{2,1,0:T(8,128)(2,1)S(1)} all-to-all(bf16[8,18,128]{2,1,0:T(8,128)(2,1)S(1)} %broadcast_in_dim.219), channel_id=1, replica_groups=mesh['kv_0'=8,'kv_1'=4,'tp_0'=4,'tp_1'=2] {'tp_0','tp_1'}, dimensions={0} | all-to-all | bytes 73728 | tf_op jit(solution)/shard_map/all_to_all | solution.py:45
  246.9 13.0 %all_to_all.123 = bf16[32,18,128]{2,1,0:T(8,128)(2,1)S(1)} all-to-all(bf16[32,18,128]{2,1,0:T(8,128)(2,1)S(1)} %broadcast_in_dim.220), channel_id=1, replica_groups=mesh['kv_0'=8,'kv_1'=4,'tp_0'=4,'tp_1'=2] {'kv_0','kv_1'}, dimensions={0} | all-to-all | bytes 294912 | tf_op jit(solution)/shard_map/all_to_all | solution.py:45
  260.5 0.3 multiply_reduce_fusion.1
  261.1 0.6 fusion.3
  261.7 0.3 reshape_reshape_reshape.9
  262.1 13.2 %all_to_all.124 = f32[8,32,288]{2,1,0:T(8,128)S(1)} all-to-all(f32[8,32,288]{2,1,0:T(8,128)S(1)} %bitcast.171), channel_id=1, replica_groups=mesh['kv_0'=8,'kv_1'=4,'tp_0'=4,'tp_1'=2] {'tp_0','tp_1'}, dimensions={0} | all-to-all | bytes 589824 | tf_op jit(solution)/shard_map/all_to_all | solution.py:24
  275.3 11.8 %all_to_all.125 = f32[32,1,288]{2,1,0:T(1,128)S(1)} all-to-all(f32[32,1,288]{2,1,0:T(1,128)S(1)} %all_to_all.93), channel_id=1, replica_groups=mesh['kv_0'=8,'kv_1'=4,'tp_0'=4,'tp_1'=2] {'kv_0','kv_1'}, dimensions={0} | all-to-all | bytes 73728 | tf_op jit(solution)/shard_map/all_to_all | solution.py:32
  287.2 0.8 reduce.125
  288.1 11.7 %all_to_all.126 = bf16[32,2,144]{2,1,0:T(2,128)(2,1)S(1)} all-to-all(bf16[32,2,144]{2,1,0:T(2,128)(2,1)S(1)} %reshape.712), channel_id=1, replica_groups=mesh['kv_0'=8,'kv_1'=4,'tp_0'=4,'tp_1'=2] {'kv_0','kv_1'}, dimensions={0} | all-to-all | bytes 36864 | tf_op jit(solution)/shard_map/all_to_all | solution.py:45
  299.9 0.7 broadcast_in_dim.223
  300.6 6.7 %all-to-all-start.17 = ((bf16[8,32,288]{2,1,0:T(8,128)(2,1)}), bf16[8,32,288]{2,1,0:T(8,128)(2,1)S(1)}, u32[]{:S(2)}, u32[]{:S(2)}) async-start(bf16[8,32,288]{2,1,0:T(8,128)(2,1)} %broadcast_in_dim.223), calls=%async_computation.17 | async-start | bytes 393216 | tf_op jit(solution)/shard_map/all_to_all | solution.py:45
  307.4 5.8 %all-to-all-done.17 = bf16[8,32,288]{2,1,0:T(8,128)(2,1)S(1)} async-done(((bf16[8,32,288]{2,1,0:T(8,128)(2,1)}), bf16[8,32,288]{2,1,0:T(8,128)(2,1)S(1)}, u32[]{:S(2)}, u32[]{:S(2)}) %all-to-all-start.17) | async-done | bytes 147488 | tf_op jit(solution)/shard_map/all_to_all | solution.py:45
  313.3 0.3 convert_element_type.616
  313.9 0.7 copy.101
  (221 shorter events, 15.6 us)
Async XLA Ops:
  0.0 41.5 %copy-start = (bf16[44,4096]{1,0:T(8,128)(2,1)S(1)}, bf16[44,4096]{1,0:T(8,128)(2,1)}, u32[]{:S(2)}) copy-start(bf16[44,4096]{1,0:T(8,128)(2,1)} %param.20) | copy-start | bytes 1081348
  22.8 12.0 %all-to-all-start.1 = ((bf16[8,2,4608]{2,1,0:T(2,128)(2,1)}), bf16[8,2,4608]{2,1,0:T(2,128)(2,1)S(1)}, u32[]{:S(2)}, u32[]{:S(2)}) async-start(bf16[8,2,4608]{2,1,0:T(2,128)(2,1)} %reshape.696), calls=%async_computation.1 | async-start | bytes 294912 | tf_op jit(solution)/shard_map/all_to_all | solution.py:45
  40.2 53.8 %copy-start.5 = (bf16[128,512]{1,0:T(8,128)(2,1)S(1)}, bf16[128,512]{1,0:T(8,128)(2,1)}, u32[]{:S(2)}) copy-start(bf16[128,512]{1,0:T(8,128)(2,1)} %param.22) | copy-start | bytes 393220
  40.2 59.4 %copy-start.6 = (bf16[128,512]{1,0:T(8,128)(2,1)S(1)}, bf16[128,512]{1,0:T(8,128)(2,1)}, u32[]{:S(2)}) copy-start(bf16[128,512]{1,0:T(8,128)(2,1)} %param.21) | copy-start | bytes 393220
  40.2 71.9 %copy-start.7 = (bf16[128,512]{1,0:T(8,128)(2,1)S(1)}, bf16[128,512]{1,0:T(8,128)(2,1)}, u32[]{:S(2)}) copy-start(bf16[128,512]{1,0:T(8,128)(2,1)} %param.23) | copy-start | bytes 393220
  80.6 12.3 %all-to-all-start.5 = ((bf16[8,32,288]{2,1,0:T(8,128)(2,1)}), bf16[8,32,288]{2,1,0:T(8,128)(2,1)S(1)}, u32[]{:S(2)}, u32[]{:S(2)}) async-start(bf16[8,32,288]{2,1,0:T(8,128)(2,1)} %broadcast_in_dim.182), calls=%async_computation.5 | async-start | bytes 393216 | tf_op jit(solution)/shard_map/all_to_all | solution.py:45
  95.7 12.5 %all-to-all-start.8 = ((bf16[32,2,144]{2,1,0:T(2,128)(2,1)}), bf16[32,2,144]{2,1,0:T(2,128)(2,1)S(1)}, u32[]{:S(2)}, u32[]{:S(2)}) async-start(bf16[32,2,144]{2,1,0:T(2,128)(2,1)} %reshape.704), calls=%async_computation.8 | async-start | bytes 65536 | tf_op jit(solution)/shard_map/all_to_all | solution.py:76
  108.2 12.5 %all-to-all-start.6 = ((bf16[32,2,144]{2,1,0:T(2,128)(2,1)}), bf16[32,2,144]{2,1,0:T(2,128)(2,1)S(1)}, u32[]{:S(2)}, u32[]{:S(2)}) async-start(bf16[32,2,144]{2,1,0:T(2,128)(2,1)} %reshape.700), calls=%async_computation.6 | async-start | bytes 65536 | tf_op jit(solution)/shard_map/all_to_all | solution.py:76
  120.7 18.9 %all-to-all-start.10 = ((bf16[32,2,144]{2,1,0:T(2,128)(2,1)}), bf16[32,2,144]{2,1,0:T(2,128)(2,1)S(1)}, u32[]{:S(2)}, u32[]{:S(2)}) async-start(bf16[32,2,144]{2,1,0:T(2,128)(2,1)} %reshape.708), calls=%async_computation.10 | async-start | bytes 65536 | tf_op jit(solution)/shard_map/all_to_all | solution.py:76
  131.2 17.8 %copy-start.8 = (bf16[4096,8]{0,1:T(8,128)(2,1)S(1)}, bf16[4096,8]{0,1:T(8,128)(2,1)}, u32[]{:S(2)}) copy-start(bf16[4096,8]{0,1:T(8,128)(2,1)} %param.24) | copy-start | bytes 196612
  137.9 27.2 %copy-start.4 = (f32[18,8,256]{2,1,0:T(8,128)S(1)}, f32[18,8,256]{2,1,0:T(8,128)}, u32[]{:S(2)}) copy-start(f32[18,8,256]{2,1,0:T(8,128)} %param.31) | copy-start | bytes 442372
  139.6 17.8 %all-to-all-start.7 = ((bf16[32,2,144]{2,1,0:T(2,128)(2,1)}), bf16[32,2,144]{2,1,0:T(2,128)(2,1)S(1)}, u32[]{:S(2)}, u32[]{:S(2)}) async-start(bf16[32,2,144]{2,1,0:T(2,128)(2,1)} %reshape.702), calls=%async_computation.7 | async-start | bytes 65536 | tf_op jit(solution)/shard_map/all_to_all | solution.py:45
  157.4 32.4 %all-to-all-start.11 = ((bf16[32,2,144]{2,1,0:T(2,128)(2,1)}), bf16[32,2,144]{2,1,0:T(2,128)(2,1)S(1)}, u32[]{:S(2)}, u32[]{:S(2)}) async-start(bf16[32,2,144]{2,1,0:T(2,128)(2,1)} %reshape.710), calls=%async_computation.11 | async-start | bytes 65536 | tf_op jit(solution)/shard_map/all_to_all | solution.py:45
  189.8 16.6 %all-to-all-start.9 = ((bf16[32,2,144]{2,1,0:T(2,128)(2,1)}), bf16[32,2,144]{2,1,0:T(2,128)(2,1)S(1)}, u32[]{:S(2)}, u32[]{:S(2)}) async-start(bf16[32,2,144]{2,1,0:T(2,128)(2,1)} %reshape.706), calls=%async_computation.9 | async-start | bytes 65536 | tf_op jit(solution)/shard_map/all_to_all | solution.py:45
  208.3 16.2 %copy-start.9 = (bf16[512,128]{1,0:T(8,128)(2,1)S(1)}, bf16[512,128]{1,0:T(8,128)(2,1)}, u32[]{:S(2)}) copy-start(bf16[512,128]{1,0:T(8,128)(2,1)} %param.25) | copy-start | bytes 393220
  212.1 48.7 %copy-start.1 = (bf16[4096,44]{0,1:T(8,128)(2,1)S(1)}, bf16[4096,44]{0,1:T(8,128)(2,1)}, u32[]{:S(2)}) copy-start(bf16[4096,44]{0,1:T(8,128)(2,1)} %param.26) | copy-start | bytes 1081348
  222.5 38.6 %copy-start.2 = (bf16[44,4096]{1,0:T(8,128)(2,1)S(1)}, bf16[44,4096]{1,0:T(8,128)(2,1)}, u32[]{:S(2)}) copy-start(bf16[44,4096]{1,0:T(8,128)(2,1)} %param.28) | copy-start | bytes 1081348
  222.5 38.6 %copy-start.3 = (bf16[4096,44]{0,1:T(8,128)(2,1)S(1)}, bf16[4096,44]{0,1:T(8,128)(2,1)}, u32[]{:S(2)}) copy-start(bf16[4096,44]{0,1:T(8,128)(2,1)} %param.27) | copy-start | bytes 1081348
  300.6 12.6 %all-to-all-start.17 = ((bf16[8,32,288]{2,1,0:T(8,128)(2,1)}), bf16[8,32,288]{2,1,0:T(8,128)(2,1)S(1)}, u32[]{:S(2)}, u32[]{:S(2)}) async-start(bf16[8,32,288]{2,1,0:T(8,128)(2,1)} %broadcast_in_dim.223), calls=%async_computation.17 | async-start | bytes 393216 | tf_op jit(solution)/shard_map/all_to_all | solution.py:45
where the time goes:
time: 316 us; the launch traced here: 315 us
  blocking collectives  156 us (49%)
  starting transfers between devices  52.8 us (17%)
  waiting for transfers between devices  42.4 us (13%)
  local copies, waits for them, and re-layouts  39.9 us (13%)
  matrix products  11.2 us (4%)
  other arithmetic  11 us (3%)
    all_to_all x5, blocking collectives, sent_to_all(): lax.all_to_all(jnp.broadcast_to(value[None], (count, *value.shape)), axis...  78.9 us
    all_to_all x6, starting transfers between devices, sent_to_all(): lax.all_to_all(jnp.broadcast_to(value[None], (count, *value.shape)), axis...  41.3 us
    all_gather x2, blocking collectives, all_in_one(): both, at, found = (lax.all_gather(jnp.concatenate(lines), axis), 0, {})  29.5 us
    all_to_all x6, waiting for transfers between devices, sent_to_all(): lax.all_to_all(jnp.broadcast_to(value[None], (count, *value.shape)), axis...  28.6 us
    all_to_all x2, blocking collectives, sum_at_owner(): lax.all_to_all(tiles, axis, split_axis=0, concat_axis=0, tiled=True)  24.5 us
    all_to_all x2, blocking collectives, summed_rows(): lax.all_to_all(nearer, far, split_axis=0, concat_axis=0, tiled=True)  23.5 us
    unnamed x52, local copies, waits for them, and re-layouts  21.4 us
    all_to_all x3, waiting for transfers between devices, sent_and_summed(): tiles = lax.all_to_all(cut_along(value, dim, count), axis, 0, 0, tiled=True)  13.8 us
  transfers between devices with their start and end apart: 9, of which 7 were waited for; matrix products, arithmetic and copies ran while one was open for 10% of the time, Pallas kernels for 0%

commit v1 on v0

v1 whole, which is shorter than its diff:
```python
import functools

import jax
import jax.numpy as jnp
from jax import lax
from jax.experimental import pallas as pl
from jax.experimental.pallas import tpu as pltpu
from jax.sharding import PartitionSpec as P

MESH = pl.DeviceIdType.MESH
F32, BF16 = jnp.float32, jnp.bfloat16
EPS = 1e-06
HD = 64
LANES = 128
NX = 4
STAGES = 15
(T_TOK, K_TOK, R_TOKQ, R_F1, T_F1, R_QKV, K_B, K_Q, R_ATT, K_ATT, T_MIX, K_MIX, R_F2, T_F2, K_STAT) = range(STAGES)


def nt(a, b):
    return lax.dot_general(a, b, (((1,), (1,)), ((), ())), preferred_element_type=F32)


def nn(a, b):
    return jnp.dot(a, b, preferred_element_type=F32)


def lane_sum(v):
    return jnp.sum(v, axis=-1, keepdims=True)


def silu(v):
    return v / (1.0 + jnp.exp(-v))


def kernel(
    n_kv, n_tp, seqs, width,
    tok_h, gains_h, g1_h, l1_h, d1_h, wq_h, wk_h, wv_h, wf_h, wo_h, g2_h, l2_h, d2_h, ck_h, cv_h, cd_h,
    out_ref,
    tok, gains, g1, l1, d1, wq, wk, wv, wf, wo, g2, l2, d2, ck, cv, cd,
    ttok, xb, xn, piece, sq1, rq1, pf, rf, tf, sqk, rqk, bb, qb, sat, rat, ab, tm, mb, mid, pf2, rf2, tf2, stb, kept,
    load_sem, ssem, rsem,
):
    kv, tp = lax.axis_index("kv"), lax.axis_index("tp")
    nz = n_kv // NX
    zz, xx = kv // NX, kv % NX
    col = pl.multiple_of(kv * LANES, LANES)
    heads = cd.shape[1]
    groups = heads * HD // LANES

    loads = [
        pltpu.make_async_copy(h, v, load_sem.at[i])
        for i, (h, v) in enumerate(
            [(tok_h, tok), (gains_h, gains), (wq_h, wq), (wk_h, wk), (wv_h, wv), (wf_h, wf), (g1_h, g1), (l1_h, l1),
             (d1_h, d1), (ck_h, ck), (cd_h, cd), (cv_h, cv), (wo_h, wo), (g2_h, g2), (l2_h, l2), (d2_h, d2)]
        )
    ]
    for copy in loads:
        copy.start()

    def owner_of(b):
        return (n_kv * b + seqs - 1) // seqs

    my_seq = (kv * seqs) // n_kv
    owns = owner_of(my_seq) == kv

    def kv_peer(i):
        a, c = i // NX, i % NX
        dz = (nz // 2 + ((a + 1) // 2) * (1 - 2 * (a % 2)) + nz) % nz
        dx = (NX // 2 + ((c + 1) // 2) * (1 - 2 * (c % 2)) + NX) % NX
        return ((zz + dz) % nz) * NX + (xx + dx) % NX

    def tp_peer(i):
        return (tp + 1 + i) % n_tp

    def send(src, dst, stage, **where):
        pltpu.make_async_remote_copy(
            src_ref=src, dst_ref=dst, send_sem=ssem.at[stage], recv_sem=rsem.at[stage],
            device_id=where, device_id_type=MESH,
        ).start()

    def wait(sem, ref):
        pltpu.make_async_copy(ref, ref, sem).wait()

    def to_all_kv(buf, slot, stage):
        @pl.loop(0, n_kv - 1)
        def _(i):
            send(buf.at[slot], buf.at[slot], stage, kv=kv_peer(i))

    def to_all_tp(buf, stage):
        @pl.loop(0, n_tp - 1)
        def _(i):
            send(buf.at[tp], buf.at[tp], stage, tp=tp_peer(i))

    def got_kv(buf, stage):
        wait(rsem.at[stage], buf.at[pl.ds(0, n_kv - 1)])

    def got_tp(buf, stage):
        wait(rsem.at[stage], buf.at[pl.ds(0, n_tp - 1)])

    def to_kv_blocks(src, dst, stage):
        @pl.loop(0, n_kv - 1)
        def _(i):
            k = kv_peer(i)
            send(src.at[k], dst.at[kv], stage, kv=k)

        dst[kv] = src[kv]

    def send_owner(src, dst, b, stage):
        @pl.when(owner_of(b) != kv)
        def _():
            send(src.at[b], dst.at[kv], stage, kv=owner_of(b))

    def to_owners(src, dst, stage):
        @pl.loop(0, seqs)
        def _(b):
            send_owner(src, dst, b, stage)

        @pl.when(owns)
        def _():
            dst[kv] = src[my_seq]

    def got_from_owners(buf, sem):
        @pl.when(owns)
        def _():
            wait(sem, buf.at[pl.ds(0, seqs - 1)])

        @pl.when(jnp.logical_not(owns))
        def _():
            wait(sem, buf.at[pl.ds(0, seqs)])

    barrier = pltpu.get_barrier_semaphore()

    @pl.loop(0, n_kv - 1)
    def _(i):
        pl.semaphore_signal(barrier, inc=1, device_id={"kv": kv_peer(i)}, device_id_type=MESH)

    @pl.loop(0, n_tp - 1)
    def _(i):
        pl.semaphore_signal(barrier, inc=1, device_id={"tp": tp_peer(i)}, device_id_type=MESH)

    loads[0].wait()
    own_w = tok.shape[0]
    lane = lax.broadcasted_iota(jnp.int32, (own_w, LANES), 1)
    row = lax.broadcasted_iota(jnp.int32, (own_w, LANES), 0)
    place = jnp.where(lane == row + own_w * tp, 1.0, 0.0).astype(BF16)
    ttok[tp] = lax.dot_general(tok[...], place, (((0,), (0,)), ((), ())), preferred_element_type=F32).astype(BF16)

    pl.semaphore_wait(barrier, n_kv + n_tp - 2)

    to_all_tp(ttok, T_TOK)
    got_tp(ttok, T_TOK)
    tblk = functools.reduce(lambda a, k: a + ttok[k].astype(F32), range(1, n_tp), ttok[0].astype(F32))
    xb[kv] = tblk.astype(BF16)
    to_all_kv(xb, kv, K_TOK)

    for i in range(1, 6):
        loads[i].wait()

    def gain(i, k=None):
        return gains[i : i + 1, pl.ds(col, LANES)] if k is None else gains[i : i + 1, k * LANES : (k + 1) * LANES]

    lane_s = lax.broadcasted_iota(jnp.int32, (seqs, LANES), 1)

    def projections(x, stats, out):
        parts = [nn(x, w[...]) for w in (wq, wk, wv)]
        for i, part in enumerate(parts):
            for j in range(groups):
                piece[:, i * groups + j, :] = part[:, j * LANES : (j + 1) * LANES]
        gates = nt(x, wf[:, pl.ds(col, LANES)])
        for j in range(groups):
            line = jnp.where(lane_s == 0, gates[:, 2 * j : 2 * j + 1], 0.0)
            line = line + jnp.where(lane_s == HD, gates[:, 2 * j + 1 : 2 * j + 2], 0.0)
            if j == 0:
                for n, stat in enumerate(stats):
                    high = stat.astype(BF16).astype(F32)
                    line = line + jnp.where(lane_s == n + 1, high, 0.0)
                    line = line + jnp.where(lane_s == HD + n + 1, stat - high, 0.0)
            piece[:, 3 * groups + j, :] = line
        out[...] = piece[...].astype(BF16)

    projections((tblk * gain(2)).astype(BF16), [lane_sum(tblk * tblk)], sq1)
    to_owners(sq1, rq1, R_TOKQ)

    def feed_forward(gate_w, lift_w, down_w, part_out):
        x = xn[...]
        act = (silu(nt(x, gate_w[...])) * nt(x, lift_w[...])).astype(BF16)
        for c in range(0, n_kv, 4):
            part = nn(act, down_w[:, c * LANES : (c + 4) * LANES])
            for j in range(4):
                part_out[c + j] = part[:, j * LANES : (j + 1) * LANES].astype(BF16)

    def block_sum(buf):
        total = buf[0].astype(F32)
        for k in range(1, n_kv):
            total = total + buf[k].astype(F32)
        return total

    def tp_sum(buf):
        return functools.reduce(lambda a, k: a + buf[k].astype(F32), range(1, n_tp), buf[0].astype(F32))

    got_kv(xb, K_TOK)
    squares = jnp.zeros((seqs, LANES), F32)
    for k in range(n_kv):
        v = xb[k].astype(F32)
        squares = squares + v * v
    scale = lax.rsqrt(lane_sum(squares) / width + EPS)
    for k in range(n_kv):
        xn[:, k * LANES : (k + 1) * LANES] = (xb[k].astype(F32) * scale * gain(0, k)).astype(BF16)
    for i in range(6, 9):
        loads[i].wait()
    feed_forward(g1, l1, d1, pf)
    to_kv_blocks(pf, rf, R_F1)
    got_kv(rf, R_F1)
    tf[tp] = block_sum(rf).astype(BF16)
    to_all_tp(tf, T_F1)
    got_tp(tf, T_F1)
    bblk = tp_sum(tf).astype(BF16)
    bb[kv] = bblk
    bf = bblk.astype(F32)
    u = bf * gain(1)
    projections((u * gain(2)).astype(BF16), [lane_sum(bf * bf), lane_sum(tblk * u), lane_sum(u * u)], sqk)
    to_owners(sqk, rqk, R_QKV)
    to_all_kv(bb, kv, K_B)

    low = lax.broadcasted_iota(jnp.int32, (groups, LANES), 1) < HD

    def halves(a, b):
        return jnp.where(low, a, b)

    lane_1 = lax.broadcasted_iota(jnp.int32, (1, LANES), 1)

    def stat_of(line, n):
        return lane_sum(jnp.where((lane_1 == n + 1) | (lane_1 == HD + n + 1), line, 0.0))

    def own_rows():
        asum, bsum = block_sum(rq1), block_sum(rqk)
        at, bt = 3 * groups, 3 * groups + 1
        s_b, s_tu, s_uu = [stat_of(bsum[at:bt], n) for n in range(3)]
        r1 = lax.rsqrt(s_b / width + EPS)
        s_mid = stat_of(asum[at:bt], 0) + r1 * s_tu + 0.25 * r1 * r1 * s_uu
        scale_mid = lax.rsqrt(s_mid / width + EPS)
        full = scale_mid * (asum + 0.5 * r1 * bsum)
        q, k, v, f = [full[i * groups : (i + 1) * groups] for i in range(4)]
        q, k, v = [t.astype(BF16).astype(F32) for t in (q, k, v)]
        f = halves(f[:, 0:1], f[:, HD : HD + 1])
        forget = jnp.minimum(f, 0.0) - jnp.log(1.0 + jnp.exp(-jnp.abs(f)))
        qk = q * k
        own = halves(lane_sum(jnp.where(low, qk, 0.0)), lane_sum(jnp.where(low, 0.0, qk))) * (HD**-0.5) - forget
        return q, own, v

    @pl.when(owns)
    def _():
        got_kv(rq1, R_TOKQ)
        got_kv(rqk, R_QKV)
        q, own, v = own_rows()
        qb[my_seq] = q
        kept[0] = own
        kept[1] = v
        to_all_kv(qb, my_seq, K_Q)

    got_from_owners(qb, rsem.at[K_Q])

    for i in range(9, 12):
        loads[i].wait()
    head_i = lax.broadcasted_iota(jnp.int32, (heads, LANES), 0)
    lane_h = lax.broadcasted_iota(jnp.int32, (heads, LANES), 1)
    masks = [head_i == 2 * j + lane_h // HD for j in range(groups)]

    @pl.loop(0, seqs)
    def _(b):
        rows = [jnp.where(masks[j], jnp.broadcast_to(qb[b, j : j + 1, :], (heads, LANES)), 0.0) for j in range(groups)]
        query = jnp.concatenate(rows, axis=1).astype(BF16)
        score = nt(query, ck[b]) * (HD**-0.5) + cd[b]
        peak = jnp.max(score, axis=1, keepdims=True)
        raised = jnp.exp(score - peak)
        total = lane_sum(raised)
        o = nn(raised.astype(BF16), cv[b]) / total
        level = jnp.broadcast_to(peak + jnp.log(total), (heads, LANES))
        for j in range(groups):
            oj = jnp.where(masks[j], o[:, j * LANES : (j + 1) * LANES], 0.0)
            sat[b, j : j + 1, :] = jnp.sum(oj, axis=0, keepdims=True)
            lj = jnp.where(masks[j], level, 0.0)
            sat[b, groups + j : groups + j + 1, :] = jnp.sum(lj, axis=0, keepdims=True)
        send_owner(sat, rat, b, R_ATT)

    @pl.when(owns)
    def _():
        rat[kv] = sat[my_seq]
        got_kv(rat, R_ATT)
        own_keep, v_keep = kept[0], kept[1]
        levels = rat[:, groups : 2 * groups, :]
        top = jnp.maximum(jnp.max(levels, axis=0), own_keep)
        share = jnp.exp(levels - top[None])
        mine = jnp.exp(own_keep - top)
        upper = jnp.sum(share * rat[:, 0:groups, :], axis=0) + mine * v_keep
        joined = upper / (jnp.sum(share, axis=0) + mine)
        ab[my_seq] = joined.astype(BF16).astype(F32)
        to_all_kv(ab, my_seq, K_ATT)

    got_kv(bb, K_B)
    squares = jnp.zeros((seqs, LANES), F32)
    for k in range(n_kv):
        v = bb[k].astype(F32)
        squares = squares + v * v
    scale = 0.5 * lax.rsqrt(lane_sum(squares) / width + EPS)
    for k in range(n_kv):
        mid[k] = xb[k].astype(F32) + bb[k].astype(F32) * scale * gain(1, k)
    loads[12].wait()

    got_from_owners(ab, rsem.at[K_ATT])
    attended = jnp.concatenate([ab[0:seqs, j, :] for j in range(groups)], axis=1).astype(BF16)
    tm[tp] = nn(attended, wo[...]).astype(BF16)
    to_all_tp(tm, T_MIX)
    got_tp(tm, T_MIX)
    mb[kv] = tp_sum(tm).astype(BF16)
    to_all_kv(mb, kv, K_MIX)
    got_kv(mb, K_MIX)

    squares = jnp.zeros((seqs, LANES), F32)
    for k in range(n_kv):
        v = mb[k].astype(F32)
        squares = squares + v * v
    scale = lax.rsqrt(lane_sum(squares) / width + EPS)
    squares = jnp.zeros((seqs, LANES), F32)
    for k in range(n_kv):
        v = mid[k] + mb[k].astype(F32) * scale * gain(3, k)
        mid[k] = v
        squares = squares + v * v
    scale = lax.rsqrt(lane_sum(squares) / width + EPS)
    for k in range(n_kv):
        xn[:, k * LANES : (k + 1) * LANES] = (mid[k] * scale * gain(4, k)).astype(BF16)
    for i in range(13, 16):
        loads[i].wait()
    feed_forward(g2, l2, d2, pf2)
    to_kv_blocks(pf2, rf2, R_F2)
    got_kv(rf2, R_F2)
    tf2[tp] = block_sum(rf2).astype(BF16)
    to_all_tp(tf2, T_F2)
    got_tp(tf2, T_F2)
    bf = tp_sum(tf2).astype(BF16).astype(F32)

    eye = lax.broadcasted_iota(jnp.int32, (seqs, LANES), 0) == lane_s
    stb[kv] = jnp.sum(jnp.where(eye, lane_sum(bf * bf), 0.0), axis=0, keepdims=True)
    to_all_kv(stb, kv, K_STAT)
    got_kv(stb, K_STAT)
    line = functools.reduce(lambda a, k: a + stb[k], range(1, n_kv), stb[0])
    total = lane_sum(jnp.where(eye, jnp.broadcast_to(line, (seqs, LANES)), 0.0))
    scale = lax.rsqrt(total / width + EPS)
    final = (mid[kv] + 0.5 * (bf * scale * gain(5))).astype(BF16)
    out_ref[...] = nt(place, final).astype(BF16)

    for stage, buf in ((T_TOK, ttok), (T_F1, tf), (T_MIX, tm), (T_F2, tf2)):
        wait(ssem.at[stage], buf.at[pl.ds(0, n_tp - 1)])
    for stage, buf in ((K_TOK, xb), (R_F1, pf), (K_B, bb), (K_MIX, mb), (R_F2, pf2), (K_STAT, stb)):
        wait(ssem.at[stage], buf.at[pl.ds(0, n_kv - 1)])
    for stage, buf in ((R_TOKQ, sq1), (R_QKV, sqk), (R_ATT, sat)):
        got_from_owners(buf, ssem.at[stage])

    @pl.when(owns)
    def _():
        for stage, buf in ((K_Q, qb), (K_ATT, ab)):
            wait(ssem.at[stage], buf.at[pl.ds(0, n_kv - 1)])


def solution(mesh):
    n_kv, n_tp = mesh.shape["kv"], mesh.shape["tp"]
    axes = ("kv", "tp")

    def body(tokens, gains, g1, l1, d1, wq, wk, wv, wf, wo, g2, l2, d2, ck, cv, cd):
        seqs, own = tokens.shape
        width = own * n_kv * n_tp
        groups = cd.shape[1] * HD // LANES
        arrays = (tokens.T, gains, g1.T, l1.T, d1, wq, wk, wv, wf.T, wo, g2.T, l2.T, d2, ck, cv, cd)
        vm = pltpu.VMEM
        block = (seqs, LANES)
        pieces = (4 * groups, LANES)
        scratch = [vm(a.shape, a.dtype) for a in arrays] + [
            vm((n_tp, *block), BF16),
            vm((n_kv, *block), BF16),
            vm((seqs, width), BF16),
            vm((seqs, *pieces), F32),
            vm((seqs, *pieces), BF16),
            vm((n_kv, *pieces), BF16),
            vm((n_kv, *block), BF16),
            vm((n_kv, *block), BF16),
            vm((n_tp, *block), BF16),
            vm((seqs, *pieces), BF16),
            vm((n_kv, *pieces), BF16),
            vm((n_kv, *block), BF16),
            vm((n_kv, groups, LANES), F32),
            vm((seqs, 2 * groups, LANES), F32),
            vm((n_kv, 2 * groups, LANES), F32),
            vm((n_kv, groups, LANES), F32),
            vm((n_tp, *block), BF16),
            vm((n_kv, *block), BF16),
            vm((n_kv, *block), F32),
            vm((n_kv, *block), BF16),
            vm((n_kv, *block), BF16),
            vm((n_tp, *block), BF16),
            vm((n_kv, 1, LANES), F32),
            vm((2, groups, LANES), F32),
            pltpu.SemaphoreType.DMA((len(arrays),)),
            pltpu.SemaphoreType.DMA((STAGES,)),
            pltpu.SemaphoreType.DMA((STAGES,)),
        ]
        out = pl.pallas_call(
            functools.partial(kernel, n_kv, n_tp, seqs, width),
            out_shape=jax.ShapeDtypeStruct((own, seqs), BF16),
            in_specs=[pl.BlockSpec(memory_space=pl.ANY)] * len(arrays),
            out_specs=pl.BlockSpec(memory_space=pltpu.VMEM),
            scratch_shapes=scratch,
            compiler_params=pltpu.CompilerParams(
                collective_id=0, has_side_effects=True, vmem_limit_bytes=56 * 1024 * 1024
            ),
            name="layer",
        )(*arrays)
        return out.T

    placed = (
        P(None, axes), P(), P(None, axes), P(None, axes), P(axes, None), P("kv", "tp"), P("kv", "tp"), P("kv", "tp"),
        P(None, "tp"), P("tp", "kv"), P(None, axes), P(None, axes), P(axes, None), P(None, "kv", "tp"),
        P(None, "kv", "tp"), P(None, "tp", "kv"),
    )
    return jax.shard_map(body, mesh=mesh, in_specs=placed, out_specs=P(None, axes), check_vma=False)
```

time: 316 us -> 101 us (0.32)
  blocking collectives: 156 us -> 0 us
  Pallas kernels: 0 us -> 99.2 us
  starting transfers between devices: 52.8 us -> 0 us
  waiting for transfers between devices: 42.4 us -> 0 us
  local copies, waits for them, and re-layouts: 39.9 us -> 1.28 us
  matrix products: 11.2 us -> 0 us
  other arithmetic: 11 us -> 0 us
    all_to_all x9 -> x0, blocking collectives: 127 us -> none  [the longest x5 78.9 us: sent_to_all(): lax.all_to_all(jnp.broadcast_to(value[None], (count, *value.shape)), axis...]
    pallas_call x0 -> x1, Pallas kernels: none -> 99.2 us  [body(): pl.pallas_call(functools.partial(kernel, n_kv, n_tp, seqs, width), out_sh...]
    all_to_all x9 -> x0, starting transfers between devices: 52.8 us -> none  [the longest x6 41.3 us: sent_to_all(): lax.all_to_all(jnp.broadcast_to(value[None], (count, *value.shape)), axis...]
    all_to_all x9 -> x0, waiting for transfers between devices: 42.4 us -> none  [the longest x6 28.6 us: sent_to_all(): lax.all_to_all(jnp.broadcast_to(value[None], (count, *value.shape)), axis...]
    all_gather x2 -> x0, blocking collectives: 29.5 us -> none  [all_in_one(): both, at, found = (lax.all_gather(jnp.concatenate(lines), axis), 0, {})]
    unnamed x52 -> x1, local copies, waits for them, and re-layouts: 21.4 us -> 1.28 us
    dot_general x11 -> x0, matrix products: 11.2 us -> none  [the longest x1 3.65 us: body(): jnp.einsum('bhp,bphd->bhd', raised.astype(jnp.bfloat16), value_heads, pre...]
    convert_element_type x36 -> x0, local copies, waits for them, and re-layouts: 7.61 us -> none  [the longest x2 3.67 us: body(): gathered_by_axis(tokens, (('kv_0', 'kv_1'), ('tp_0', 'tp_1')), 1)]
  transfers between devices with their start and end apart: 9 -> 0, of which waited for: 7 -> 0; matrix products, arithmetic and copies ran while one was open for 10% -> 0% of each run, Pallas kernels for 0% -> 0%
where the time goes in v1:
time: 101 us
  Pallas kernels  99.2 us (98%)
  local copies, waits for them, and re-layouts  1.28 us (1%)
    pallas_call x1, Pallas kernels, body(): pl.pallas_call(functools.partial(kernel, n_kv, n_tp, seqs, width), out_sh...  99.2 us

profile of v1, /device:TPU:1, one launch (start us, length us, event | category | flops | bytes accessed | tf_op | source)
XLA Modules:
  0.0 100.5 jit_solution(8168364118693375215)
XLA Ops:
  0.0 99.2 %layer.1 = bf16[16,18]{1,0:T(8,128)(2,1)} custom-call(bf16[16,18]{1,0:T(8,128)(2,1)} %bitcast.13, f32[6,4096]{1,0:T(8,128)} %gains_h.1, bf16[44,4096]{1,0:T(8,128)(2,1)} %bitcast.7, bf16[44,4096]{1,0:T(8,128)(2,1)} %bitcast.8, bf16[44,4096]{1,0:T(8,128)(2,1)} %d1_h.1, bf16[128,512]{1,0:T(8,128)(2,1)} %wq_h.1, bf16[128,512]{1,0:T(8,128)(2,1)} %wk_h.1, ...), custom_call_target="tpu_custom_call" | custom-call | tf_op jit(solution)/shard_map/layer/pallas_call | solution.py:407
  99.2 1.3 %copy.18 = bf16[18,16]{0,1:T(8,128)(2,1)} copy(bf16[18,16]{0,1:T(8,128)(2,1)} %bitcast.12) | data formatting | bytes 1152

commit v2 on v1

--- a/solution.py
+++ b/solution.py
@@ -12,6 +12,7 @@
 EPS = 1e-06
 HD = 64
 LANES = 128
+ROWS = 24
 NX = 4
 STAGES = 15
 (T_TOK, K_TOK, R_TOKQ, R_F1, T_F1, R_QKV, K_B, K_Q, R_ATT, K_ATT, T_MIX, K_MIX, R_F2, T_F2, K_STAT) = range(STAGES)
@@ -27,6 +28,18 @@
 
 def lane_sum(v):
     return jnp.sum(v, axis=-1, keepdims=True)
+
+
+def rows_of(ref, k):
+    return ref[k].astype(F32).reshape(ROWS, LANES)
+
+
+def put_rows(ref, k, v):
+    ref[k] = v.reshape(ROWS // 8, 8, LANES).astype(BF16)
+
+
+def padded(v):
+    return jnp.concatenate([v, jnp.zeros((ROWS - v.shape[0], v.shape[1]), v.dtype)], axis=0)
 
 
 def silu(v):
@@ -38,7 +51,7 @@
     tok_h, gains_h, g1_h, l1_h, d1_h, wq_h, wk_h, wv_h, wf_h, wo_h, g2_h, l2_h, d2_h, ck_h, cv_h, cd_h,
     out_ref,
     tok, gains, g1, l1, d1, wq, wk, wv, wf, wo, g2, l2, d2, ck, cv, cd,
-    ttok, xb, xn, piece, sq1, rq1, pf, rf, tf, sqk, rqk, bb, qb, sat, rat, ab, tm, mb, mid, pf2, rf2, tf2, stb, kept,
+    ttok, xb, xn, piece, sq1, rq1, pf, rf, tf, sqk, rqk, bb, qb, sat, rat, ab, tm, mb, mid, pf2, rf2, tf2, stb, kept, sc, wt, sl, si,
     load_sem, ssem, rsem,
 ):
     kv, tp = lax.axis_index("kv"), lax.axis_index("tp")
@@ -144,14 +157,24 @@
     lane = lax.broadcasted_iota(jnp.int32, (own_w, LANES), 1)
     row = lax.broadcasted_iota(jnp.int32, (own_w, LANES), 0)
     place = jnp.where(lane == row + own_w * tp, 1.0, 0.0).astype(BF16)
-    ttok[tp] = lax.dot_general(tok[...], place, (((0,), (0,)), ((), ())), preferred_element_type=F32).astype(BF16)
+    put_rows(ttok, tp, padded(lax.dot_general(tok[...], place, (((0,), (0,)), ((), ())), preferred_element_type=F32)))
+    ab[seqs:ROWS] = jnp.zeros((ROWS - seqs, groups, LANES), F32)
 
     pl.semaphore_wait(barrier, n_kv + n_tp - 2)
+
+    def block_sum(buf):
+        return functools.reduce(lambda a, k: a + rows_of(buf, k), range(1, n_kv), rows_of(buf, 0))
+
+    def tp_sum(buf):
+        return functools.reduce(lambda a, k: a + rows_of(buf, k), range(1, n_tp), rows_of(buf, 0))
+
+    def piece_sum(buf):
+        return functools.reduce(lambda a, k: a + buf[k].astype(F32), range(1, n_kv), buf[0].astype(F32))
 
     to_all_tp(ttok, T_TOK)
     got_tp(ttok, T_TOK)
-    tblk = functools.reduce(lambda a, k: a + ttok[k].astype(F32), range(1, n_tp), ttok[0].astype(F32))
-    xb[kv] = tblk.astype(BF16)
+    tblk = tp_sum(ttok)
+    put_rows(xb, kv, tblk)
     to_all_kv(xb, kv, K_TOK)
 
     for i in range(1, 6):
@@ -160,13 +183,13 @@
     def gain(i, k=None):
         return gains[i : i + 1, pl.ds(col, LANES)] if k is None else gains[i : i + 1, k * LANES : (k + 1) * LANES]
 
-    lane_s = lax.broadcasted_iota(jnp.int32, (seqs, LANES), 1)
+    lane_s = lax.broadcasted_iota(jnp.int32, (ROWS, LANES), 1)
 
     def projections(x, stats, out):
         parts = [nn(x, w[...]) for w in (wq, wk, wv)]
         for i, part in enumerate(parts):
             for j in range(groups):
-                piece[:, i * groups + j, :] = part[:, j * LANES : (j + 1) * LANES]
+                piece[:, i * groups + j, :] = part[0:seqs, j * LANES : (j + 1) * LANES]
         gates = nt(x, wf[:, pl.ds(col, LANES)])
         for j in range(groups):
             line = jnp.where(lane_s == 0, gates[:, 2 * j : 2 * j + 1], 0.0)
@@ -176,7 +199,7 @@
                     high = stat.astype(BF16).astype(F32)
                     line = line + jnp.where(lane_s == n + 1, high, 0.0)
                     line = line + jnp.where(lane_s == HD + n + 1, stat - high, 0.0)
-            piece[:, 3 * groups + j, :] = line
+            piece[:, 3 * groups + j, :] = line[0:seqs]
         out[...] = piece[...].astype(BF16)
 
     projections((tblk * gain(2)).astype(BF16), [lane_sum(tblk * tblk)], sq1)
@@ -188,40 +211,29 @@
         for c in range(0, n_kv, 4):
             part = nn(act, down_w[:, c * LANES : (c + 4) * LANES])
             for j in range(4):
-                part_out[c + j] = part[:, j * LANES : (j + 1) * LANES].astype(BF16)
-
-    def block_sum(buf):
-        total = buf[0].astype(F32)
-        for k in range(1, n_kv):
-            total = total + buf[k].astype(F32)
-        return total
-
-    def tp_sum(buf):
-        return functools.reduce(lambda a, k: a + buf[k].astype(F32), range(1, n_tp), buf[0].astype(F32))
+                put_rows(part_out, c + j, part[:, j * LANES : (j + 1) * LANES])
 
     got_kv(xb, K_TOK)
-    squares = jnp.zeros((seqs, LANES), F32)
-    for k in range(n_kv):
-        v = xb[k].astype(F32)
+    squares = jnp.zeros((ROWS, LANES), F32)
+    for k in range(n_kv):
+        v = rows_of(xb, k)
         squares = squares + v * v
     scale = lax.rsqrt(lane_sum(squares) / width + EPS)
     for k in range(n_kv):
-        xn[:, k * LANES : (k + 1) * LANES] = (xb[k].astype(F32) * scale * gain(0, k)).astype(BF16)
+        xn[:, k * LANES : (k + 1) * LANES] = (rows_of(xb, k) * scale * gain(0, k)).astype(BF16)
     for i in range(6, 9):
         loads[i].wait()
     feed_forward(g1, l1, d1, pf)
     to_kv_blocks(pf, rf, R_F1)
     got_kv(rf, R_F1)
-    tf[tp] = block_sum(rf).astype(BF16)
+    put_rows(tf, tp, block_sum(rf))
     to_all_tp(tf, T_F1)
     got_tp(tf, T_F1)
-    bblk = tp_sum(tf).astype(BF16)
-    bb[kv] = bblk
-    bf = bblk.astype(F32)
+    put_rows(bb, kv, tp_sum(tf))
+    bf = rows_of(bb, kv)
     u = bf * gain(1)
     projections((u * gain(2)).astype(BF16), [lane_sum(bf * bf), lane_sum(tblk * u), lane_sum(u * u)], sqk)
     to_owners(sqk, rqk, R_QKV)
-    to_all_kv(bb, kv, K_B)
 
     low = lax.broadcasted_iota(jnp.int32, (groups, LANES), 1) < HD
 
@@ -234,7 +246,7 @@
         return lane_sum(jnp.where((lane_1 == n + 1) | (lane_1 == HD + n + 1), line, 0.0))
 
     def own_rows():
-        asum, bsum = block_sum(rq1), block_sum(rqk)
+        asum, bsum = piece_sum(rq1), piece_sum(rqk)
         at, bt = 3 * groups, 3 * groups + 1
         s_b, s_tu, s_uu = [stat_of(bsum[at:bt], n) for n in range(3)]
         r1 = lax.rsqrt(s_b / width + EPS)
@@ -260,6 +272,7 @@
         to_all_kv(qb, my_seq, K_Q)
 
     got_from_owners(qb, rsem.at[K_Q])
+    to_all_kv(bb, kv, K_B)
 
     for i in range(9, 12):
         loads[i].wait()
@@ -267,22 +280,36 @@
     lane_h = lax.broadcasted_iota(jnp.int32, (heads, LANES), 1)
     masks = [head_i == 2 * j + lane_h // HD for j in range(groups)]
 
-    @pl.loop(0, seqs)
-    def _(b):
-        rows = [jnp.where(masks[j], jnp.broadcast_to(qb[b, j : j + 1, :], (heads, LANES)), 0.0) for j in range(groups)]
-        query = jnp.concatenate(rows, axis=1).astype(BF16)
-        score = nt(query, ck[b]) * (HD**-0.5) + cd[b]
-        peak = jnp.max(score, axis=1, keepdims=True)
-        raised = jnp.exp(score - peak)
-        total = lane_sum(raised)
-        o = nn(raised.astype(BF16), cv[b]) / total
-        level = jnp.broadcast_to(peak + jnp.log(total), (heads, LANES))
-        for j in range(groups):
-            oj = jnp.where(masks[j], o[:, j * LANES : (j + 1) * LANES], 0.0)
-            sat[b, j : j + 1, :] = jnp.sum(oj, axis=0, keepdims=True)
-            lj = jnp.where(masks[j], level, 0.0)
-            sat[b, groups + j : groups + j + 1, :] = jnp.sum(lj, axis=0, keepdims=True)
-        send_owner(sat, rat, b, R_ATT)
+    batch = 6
+
+    @pl.loop(0, seqs, step=batch)
+    def _(first):
+        for i in range(batch):
+            b = first + i
+            rows = [jnp.where(masks[j], jnp.broadcast_to(qb[b, j : j + 1, :], (heads, LANES)), 0.0) for j in range(groups)]
+            query = jnp.concatenate(rows, axis=1).astype(BF16)
+            sc[b] = nt(query, ck[b]) * (HD**-0.5) + cd[b]
+
+    score = sc[...]
+    peak = jnp.max(score, axis=2, keepdims=True)
+    raised = jnp.exp(score - peak)
+    total = jnp.sum(raised, axis=2, keepdims=True)
+    wt[...] = raised.astype(BF16)
+    sl[...] = jnp.broadcast_to(peak + jnp.log(total), (seqs, heads, LANES))
+    si[...] = jnp.broadcast_to(1.0 / total, (seqs, heads, LANES))
+
+    @pl.loop(0, seqs, step=batch)
+    def _(first):
+        for i in range(batch):
+            b = first + i
+            o = nn(wt[b], cv[b])
+            level, part = sl[b], si[b]
+            for j in range(groups):
+                oj = jnp.where(masks[j], o[:, j * LANES : (j + 1) * LANES] * part, 0.0)
+                sat[b, j : j + 1, :] = jnp.sum(oj, axis=0, keepdims=True)
+                lj = jnp.where(masks[j], level, 0.0)
+                sat[b, groups + j : groups + j + 1, :] = jnp.sum(lj, axis=0, keepdims=True)
+            send_owner(sat, rat, b, R_ATT)
 
     @pl.when(owns)
     def _():
@@ -299,32 +326,32 @@
         to_all_kv(ab, my_seq, K_ATT)
 
     got_kv(bb, K_B)
-    squares = jnp.zeros((seqs, LANES), F32)
-    for k in range(n_kv):
-        v = bb[k].astype(F32)
+    squares = jnp.zeros((ROWS, LANES), F32)
+    for k in range(n_kv):
+        v = rows_of(bb, k)
         squares = squares + v * v
     scale = 0.5 * lax.rsqrt(lane_sum(squares) / width + EPS)
     for k in range(n_kv):
-        mid[k] = xb[k].astype(F32) + bb[k].astype(F32) * scale * gain(1, k)
+        mid[k] = rows_of(xb, k) + rows_of(bb, k) * scale * gain(1, k)
     loads[12].wait()
 
     got_from_owners(ab, rsem.at[K_ATT])
-    attended = jnp.concatenate([ab[0:seqs, j, :] for j in range(groups)], axis=1).astype(BF16)
-    tm[tp] = nn(attended, wo[...]).astype(BF16)
+    attended = jnp.concatenate([ab[0:ROWS, j, :] for j in range(groups)], axis=1).astype(BF16)
+    put_rows(tm, tp, nn(attended, wo[...]))
     to_all_tp(tm, T_MIX)
     got_tp(tm, T_MIX)
-    mb[kv] = tp_sum(tm).astype(BF16)
+    put_rows(mb, kv, tp_sum(tm))
     to_all_kv(mb, kv, K_MIX)
     got_kv(mb, K_MIX)
 
-    squares = jnp.zeros((seqs, LANES), F32)
-    for k in range(n_kv):
-        v = mb[k].astype(F32)
+    squares = jnp.zeros((ROWS, LANES), F32)
+    for k in range(n_kv):
+        v = rows_of(mb, k)
         squares = squares + v * v
     scale = lax.rsqrt(lane_sum(squares) / width + EPS)
-    squares = jnp.zeros((seqs, LANES), F32)
-    for k in range(n_kv):
-        v = mid[k] + mb[k].astype(F32) * scale * gain(3, k)
+    squares = jnp.zeros((ROWS, LANES), F32)
+    for k in range(n_kv):
+        v = mid[k] + rows_of(mb, k) * scale * gain(3, k)
         mid[k] = v
         squares = squares + v * v
     scale = lax.rsqrt(lane_sum(squares) / width + EPS)
@@ -335,20 +362,20 @@
     feed_forward(g2, l2, d2, pf2)
     to_kv_blocks(pf2, rf2, R_F2)
     got_kv(rf2, R_F2)
-    tf2[tp] = block_sum(rf2).astype(BF16)
+    put_rows(tf2, tp, block_sum(rf2))
     to_all_tp(tf2, T_F2)
     got_tp(tf2, T_F2)
-    bf = tp_sum(tf2).astype(BF16).astype(F32)
-
-    eye = lax.broadcasted_iota(jnp.int32, (seqs, LANES), 0) == lane_s
+    bf = tp_sum(tf2)
+
+    eye = lax.broadcasted_iota(jnp.int32, (ROWS, LANES), 0) == lane_s
     stb[kv] = jnp.sum(jnp.where(eye, lane_sum(bf * bf), 0.0), axis=0, keepdims=True)
     to_all_kv(stb, kv, K_STAT)
     got_kv(stb, K_STAT)
     line = functools.reduce(lambda a, k: a + stb[k], range(1, n_kv), stb[0])
-    total = lane_sum(jnp.where(eye, jnp.broadcast_to(line, (seqs, LANES)), 0.0))
+    total = lane_sum(jnp.where(eye, jnp.broadcast_to(line, (ROWS, LANES)), 0.0))
     scale = lax.rsqrt(total / width + EPS)
     final = (mid[kv] + 0.5 * (bf * scale * gain(5))).astype(BF16)
-    out_ref[...] = nt(place, final).astype(BF16)
+    out_ref[...] = nt(place, final)[:, 0:seqs].astype(BF16)
 
     for stage, buf in ((T_TOK, ttok), (T_F1, tf), (T_MIX, tm), (T_F2, tf2)):
         wait(ssem.at[stage], buf.at[pl.ds(0, n_tp - 1)])
@@ -373,12 +400,13 @@
         groups = cd.shape[1] * HD // LANES
         arrays = (tokens.T, gains, g1.T, l1.T, d1, wq, wk, wv, wf.T, wo, g2.T, l2.T, d2, ck, cv, cd)
         vm = pltpu.VMEM
-        block = (seqs, LANES)
+        block = (ROWS // 8, 8, LANES)
+        heads = cd.shape[1]
         pieces = (4 * groups, LANES)
         scratch = [vm(a.shape, a.dtype) for a in arrays] + [
             vm((n_tp, *block), BF16),
             vm((n_kv, *block), BF16),
-            vm((seqs, width), BF16),
+            vm((ROWS, width), BF16),
             vm((seqs, *pieces), F32),
             vm((seqs, *pieces), BF16),
             vm((n_kv, *pieces), BF16),
@@ -394,12 +422,16 @@
             vm((n_kv, groups, LANES), F32),
             vm((n_tp, *block), BF16),
             vm((n_kv, *block), BF16),
-            vm((n_kv, *block), F32),
+            vm((n_kv, ROWS, LANES), F32),
             vm((n_kv, *block), BF16),
             vm((n_kv, *block), BF16),
             vm((n_tp, *block), BF16),
             vm((n_kv, 1, LANES), F32),
             vm((2, groups, LANES), F32),
+            vm((seqs, heads, cd.shape[2]), F32),
+            vm((seqs, heads, cd.shape[2]), BF16),
+            vm((seqs, heads, LANES), F32),
+            vm((seqs, heads, LANES), F32),
             pltpu.SemaphoreType.DMA((len(arrays),)),
             pltpu.SemaphoreType.DMA((STAGES,)),
             pltpu.SemaphoreType.DMA((STAGES,)),

time: 101 us -> 95.1 us (0.942)
  Pallas kernels: 99.2 us -> 93.7 us
    pallas_call x1, Pallas kernels: 99.2 us -> 93.7 us  [body(): pl.pallas_call(functools.partial(kernel, n_kv, n_tp, seqs, width), out_sh...]
where the time goes in v2:
time: 95.1 us; the launch traced here: 95 us
  Pallas kernels  93.7 us (99%)
  local copies, waits for them, and re-layouts  1.28 us (1%)
    pallas_call x1, Pallas kernels, body(): pl.pallas_call(functools.partial(kernel, n_kv, n_tp, seqs, width), out_sh...  93.7 us

profile of v2, /device:TPU:1, one launch (start us, length us, event | category | flops | bytes accessed | tf_op | source)
XLA Modules:
  0.0 95.0 jit_solution(17561905338050226673)
XLA Ops:
  0.0 93.7 %layer.1 = bf16[16,18]{1,0:T(8,128)(2,1)} custom-call(bf16[16,18]{1,0:T(8,128)(2,1)} %bitcast.13, f32[6,4096]{1,0:T(8,128)} %gains_h.1, bf16[44,4096]{1,0:T(8,128)(2,1)} %bitcast.7, bf16[44,4096]{1,0:T(8,128)(2,1)} %bitcast.8, bf16[44,4096]{1,0:T(8,128)(2,1)} %d1_h.1, bf16[128,512]{1,0:T(8,128)(2,1)} %wq_h.1, bf16[128,512]{1,0:T(8,128)(2,1)} %wk_h.1, ...), custom_call_target="tpu_custom_call" | custom-call | tf_op jit(solution)/shard_map/layer/pallas_call | solution.py:439
  93.7 1.3 %copy.18 = bf16[18,16]{0,1:T(8,128)(2,1)} copy(bf16[18,16]{0,1:T(8,128)(2,1)} %bitcast.12) | data formatting | bytes 1152

commit v3 on v2

v3 whole, which is shorter than its diff:
```python
import functools

import jax
import jax.numpy as jnp
from jax import lax
from jax.experimental import pallas as pl
from jax.experimental.pallas import tpu as pltpu
from jax.sharding import PartitionSpec as P

MESH = pl.DeviceIdType.MESH
F32, BF16 = jnp.float32, jnp.bfloat16
EPS = 1e-06
HD = 64
LANES = 128
ROWS = 24
TILE = 32
NX = 4
STAGES = 21
(T_TOK, K_TOK, X_W, X_WO, R_F1, P_F1, K_QA, K_QB, O_A, O_B, Z_ST, Z_OWN, Z_OWNL, K_B, R_ATT, R_LSE, P_MIX, K_MIX,
 R_F2, T_F2, K_STAT) = range(STAGES)


def nt(a, b):
    return lax.dot_general(a, b, (((1,), (1,)), ((), ())), preferred_element_type=F32)


def nn(a, b):
    return jnp.dot(a, b, preferred_element_type=F32)


def lane_sum(v):
    return jnp.sum(v, axis=-1, keepdims=True)


def rows_of(ref, k):
    return ref[k, 0:ROWS, :].astype(F32)


def put_rows(ref, k, v):
    ref[k, 0:ROWS, :] = v.astype(BF16)


def total_of(buf, slots):
    slots = list(slots)
    return functools.reduce(lambda a, k: a + rows_of(buf, k), slots[1:], rows_of(buf, slots[0]))


def padded(v):
    return jnp.concatenate([v, jnp.zeros((ROWS - v.shape[0], v.shape[1]), v.dtype)], axis=0)


def silu(v):
    return v / (1.0 + jnp.exp(-v))


def kernel(
    n_kv, n_tp, seqs, width,
    tok_h, gains_h, wq_h, wk_h, wv_h, wf_h, g1_h, l1_h, d1_h, ck_h, cd_h, cv_h, wo_h, g2_h, l2_h, d2_h,
    out_ref,
    tok, gains, wq, wk, wv, wf, g1, l1, d1, ck, cd, cv, wo, g2, l2, d2,
    ttok, xb, xn, wx, wo2, pf, rf, pb, bb, qa, qb, oa, ob, roa, rob, zst, qf, sc, wt, si, om, so, ls, ro, rl, wsq,
    sm, rm, mb, mid, pf2, rf2, tf2, stb,
    load_sem, ssem, rsem, hello,
):
    kv, tp = lax.axis_index("kv"), lax.axis_index("tp")
    nz = n_kv // NX
    zz, xx = kv // NX, kv % NX
    n_plane = NX * n_tp
    me = xx * n_tp + tp
    heads = cd.shape[1]
    groups = heads * HD // LANES
    zwide = NX * LANES
    zcol = pl.multiple_of(zz * zwide, LANES)
    xcol = pl.multiple_of(xx * LANES, LANES)
    col = pl.multiple_of(kv * LANES, LANES)

    loads = [
        pltpu.make_async_copy(h, v, load_sem.at[i])
        for i, (h, v) in enumerate(
            [(tok_h, tok), (gains_h, gains), (wq_h, wq), (wk_h, wk), (wv_h, wv), (wf_h, wf), (g1_h, g1), (l1_h, l1),
             (d1_h, d1), (ck_h, ck), (cd_h, cd), (cv_h, cv), (wo_h, wo), (g2_h, g2), (l2_h, l2), (d2_h, d2)]
        )
    ]
    for copy in loads:
        copy.start()

    def ordered(i, n):
        return (n // 2 + ((i + 1) // 2) * (1 - 2 * (i % 2)) + n) % n

    def kv_at(dz, dx):
        return ((zz + dz + nz) % nz) * NX + (xx + dx) % NX

    def kv_peer(i):
        return kv_at(ordered(i // NX, nz), ordered(i % NX, NX))

    def tp_peer(i):
        return (tp + 1 + i) % n_tp

    def plane_peer(i):
        return (xx + ordered(i // n_tp, NX)) % NX, (tp + 1 + i % n_tp) % n_tp

    def at(x):
        return zz * NX + x

    z_own = (2 * xx + tp) % nz
    owns = zz == z_own

    def send(src, dst, stage, **where):
        pltpu.make_async_remote_copy(
            src_ref=src, dst_ref=dst, send_sem=ssem.at[stage], recv_sem=rsem.at[stage],
            device_id=where, device_id_type=MESH,
        ).start()

    def wait(sem, ref):
        pltpu.make_async_copy(ref, ref, sem).wait()

    def part(buf, slot):
        if buf.shape[-2] != TILE:
            return buf.at[slot]
        if len(buf.shape) == 4:
            return buf.at[slot, :, pl.ds(0, seqs)]
        return buf.at[slot, pl.ds(0, seqs)]

    def got(stage, buf, n):
        wait(rsem.at[stage], part(buf, pl.ds(0, n)))

    def gone(stage, buf, n):
        wait(ssem.at[stage], part(buf, pl.ds(0, n)))

    def to_all_kv(buf, stage, count=n_kv - 1):
        @pl.loop(0, count)
        def _(i):
            send(part(buf, kv), part(buf, kv), stage, kv=kv_peer(i))

    def to_all_tp(buf, stage):
        @pl.loop(0, n_tp - 1)
        def _(i):
            send(part(buf, tp), part(buf, tp), stage, tp=tp_peer(i))

    def to_all_z(buf, slot, stage):
        @pl.loop(0, nz - 1)
        def _(i):
            send(part(buf, slot), part(buf, slot), stage, kv=kv_at(ordered(i, nz), 0))

    def to_kv_blocks(src, dst, stage):
        @pl.loop(0, n_kv - 1)
        def _(i):
            k = kv_peer(i)
            send(part(src, k), part(dst, kv), stage, kv=k)

        dst[kv] = src[kv]

    barrier = pltpu.get_barrier_semaphore()
    for i in range(n_tp - 1):
        pl.semaphore_signal(barrier, inc=1, device_id={"tp": tp_peer(i)}, device_id_type=MESH)
    for dz, dx in [(0, d) for d in range(1, NX)] + [(1, 0), (-1, 0)]:
        pl.semaphore_signal(barrier, inc=1, device_id={"kv": kv_at(dz, dx)}, device_id_type=MESH)

    loads[0].wait()
    own_w = tok.shape[0]
    lane = lax.broadcasted_iota(jnp.int32, (own_w, LANES), 1)
    row = lax.broadcasted_iota(jnp.int32, (own_w, LANES), 0)
    place = jnp.where(lane == row + own_w * tp, 1.0, 0.0).astype(BF16)
    mine = lax.dot_general(tok[...], place, (((0,), (0,)), ((), ())), preferred_element_type=F32)
    put_rows(ttok, tp, padded(mine))

    pl.semaphore_wait(barrier, n_tp - 1 + NX - 1 + 2)

    to_all_tp(ttok, T_TOK)
    for i in range(2, 5):
        loads[i].wait()
    for d in range(1, NX):
        j = (xx + d) % NX
        for m, w in enumerate((wq, wk, wv)):
            send(w.at[:, pl.ds(pl.multiple_of(j * LANES, LANES), LANES)], wx.at[m, xx], X_W, kv=at(j))
    for m, w in enumerate((wq, wk, wv)):
        wx[m, xx] = w[:, pl.ds(xcol, LANES)]
    for n, step in enumerate((1, 2, 1)):
        for dz in (step, -step):
            pl.semaphore_signal(hello.at[n], inc=1, device_id={"kv": kv_at(dz, 0)}, device_id_type=MESH)
        pl.semaphore_wait(hello.at[n], 2)
    got(T_TOK, ttok, n_tp - 1)
    put_rows(xb, kv, total_of(ttok, range(n_tp)))
    to_all_kv(xb, K_TOK)

    def gain(i, k):
        return gains[i : i + 1, k * LANES : (k + 1) * LANES]

    def zgain(i):
        return gains[i : i + 1, pl.ds(zcol, zwide)]

    def feed_forward(gate_w, lift_w, down_w, part_out):
        x = xn[...]
        act = (silu(nt(x, gate_w[...])) * nt(x, lift_w[...])).astype(BF16)
        for c in range(0, n_kv, 4):
            some = nn(act, down_w[:, c * LANES : (c + 4) * LANES])
            for j in range(4):
                put_rows(part_out, c + j, some[:, j * LANES : (j + 1) * LANES])

    lane_r = lax.broadcasted_iota(jnp.int32, (ROWS, LANES), 1)
    low = lane_r < HD
    eye = lax.broadcasted_iota(jnp.int32, (ROWS, LANES), 0) == lane_r

    def flat(column):
        return jnp.sum(jnp.where(eye, column, 0.0), axis=0, keepdims=True)

    def upright(line):
        return lane_sum(jnp.where(eye, jnp.broadcast_to(line, (ROWS, LANES)), 0.0))

    loads[1].wait()
    got(K_TOK, xb, n_kv - 1)
    squares = jnp.zeros((ROWS, LANES), F32)
    for k in range(n_kv):
        v = rows_of(xb, k)
        squares = squares + v * v
    s_tt = lane_sum(squares)
    scale = lax.rsqrt(s_tt / width + EPS)
    for k in range(n_kv):
        xn[:, k * LANES : (k + 1) * LANES] = (rows_of(xb, k) * scale * gain(0, k)).astype(BF16)
    for i in range(6, 9):
        loads[i].wait()
    feed_forward(g1, l1, d1, pf)
    to_kv_blocks(pf, rf, R_F1)

    loads[5].wait()
    wait(rsem.at[X_W], wx.at[:, pl.ds(0, NX - 1)])
    tz = jnp.concatenate([rows_of(xb, at(x)) for x in range(NX)], axis=1)
    lane_f = lax.broadcasted_iota(jnp.int32, (ROWS, heads), 1)

    def projections(x, q_out, o_out):
        q, k, v = [nn(x, wx[m].reshape(zwide, LANES)) for m in range(3)]
        f = nt(x, wf[:, pl.ds(zcol, zwide)])
        f0, f1 = [lane_sum(jnp.where(lane_f == 2 * xx + g, f, 0.0)) for g in range(2)]
        put_rows(q_out, kv, q)
        put_rows(o_out, 0, k)
        put_rows(o_out, 1, v)
        put_rows(o_out, 2, jnp.where(low, f0, f1))

    def to_owner(src, dst, stage):
        whole = src.at[:, pl.ds(0, seqs)]

        @pl.when(jnp.logical_not(owns))
        def _():
            send(whole, dst.at[zz, :, pl.ds(0, seqs)], stage, kv=z_own * NX + xx)

        @pl.when(owns)
        def _():
            dst[zz] = src[...]

    projections((tz * zgain(2)).astype(BF16), qa, oa)

    got(R_F1, rf, n_kv - 1)
    put_rows(pb, me, total_of(rf, range(n_kv)))

    def to_plane(src, dst, stage, pick):
        @pl.loop(0, n_plane - 1)
        def _(i):
            x, t = plane_peer(i)
            send(part(src, pick(x)), part(dst, me), stage, kv=at(x), tp=t)

    to_plane(pb, pb, P_F1, lambda x: me)
    to_all_kv(qa, K_QA)
    to_owner(oa, roa, O_A)

    got(P_F1, pb, n_plane - 1)
    for x in range(NX):
        put_rows(bb, at(x), total_of(pb, range(x * n_tp, (x + 1) * n_tp)))
    bz = jnp.concatenate([rows_of(bb, at(x)) for x in range(NX)], axis=1)
    u = bz * zgain(1)
    projections((u * zgain(2)).astype(BF16), qb, ob)
    to_all_kv(qb, K_QB)
    for n, stat in enumerate((bz * bz, tz * u, u * u)):
        zst[zz, n : n + 1, :] = flat(lane_sum(stat))
    to_all_z(zst, zz, Z_ST)
    to_owner(ob, rob, O_B)

    got(K_QA, qa, n_kv - 1)
    got(Z_ST, zst, nz - 1)
    stats = functools.reduce(lambda a, z: a + zst[z], range(1, nz), zst[0])
    s_bb, s_tu, s_uu = [upright(stats[n : n + 1]) for n in range(3)]
    r1 = lax.rsqrt(s_bb / width + EPS)
    half = 0.5 * r1
    scale_mid = lax.rsqrt((s_tt + r1 * s_tu + half * half * s_uu) / width + EPS)
    got(K_QB, qb, n_kv - 1)
    for j in range(groups):
        slots = range(j, n_kv, NX)
        qf[j] = (scale_mid * (total_of(qa, slots) + half * total_of(qb, slots))).astype(BF16).astype(F32)

    to_all_kv(bb, K_B, n_kv - NX)
    loads[12].wait()
    for d in range(1, NX):
        j = (xx + d) % NX
        send(wo.at[pl.ds(pl.multiple_of(j * LANES, LANES), LANES), :], wo2.at[xx], X_WO, kv=at(j))
    wo2[xx] = wo[pl.ds(xcol, LANES), :]
    for i in range(9, 12):
        loads[i].wait()
    head_i = lax.broadcasted_iota(jnp.int32, (heads, LANES), 0)
    lane_h = lax.broadcasted_iota(jnp.int32, (heads, LANES), 1)
    masks = [head_i == 2 * j + lane_h // HD for j in range(groups)]
    batch = 6

    @pl.loop(0, seqs, step=batch)
    def _(first):
        for i in range(batch):
            b = first + i
            rows = [
                jnp.where(masks[j], jnp.broadcast_to(qf[j, pl.ds(b, 1), :], (heads, LANES)), 0.0) for j in range(groups)
            ]
            query = jnp.concatenate(rows, axis=1).astype(BF16)
            sc[b] = nt(query, ck[b]) * (HD**-0.5) + cd[b]

    score = sc[...]
    peak = jnp.max(score, axis=2, keepdims=True)
    raised = jnp.exp(score - peak)
    total = jnp.sum(raised, axis=2, keepdims=True)
    wt[...] = raised.astype(BF16)
    si[...] = jnp.broadcast_to(1.0 / total, (seqs, heads, LANES))
    level = jnp.broadcast_to(peak + jnp.log(total), (seqs, heads, LANES))
    turn = lax.broadcasted_iota(jnp.int32, (seqs, heads, LANES), 0) == lax.broadcasted_iota(
        jnp.int32, (seqs, heads, LANES), 2
    )
    lines = jnp.sum(jnp.where(turn, level, 0.0), axis=0)
    for j in range(groups):
        ls[j] = lines[2 * j : 2 * j + 2]

    @pl.loop(0, seqs, step=batch)
    def _(first):
        for i in range(batch):
            b = first + i
            o = nn(wt[b], cv[b])
            share = si[b]
            here = pl.ds(pl.multiple_of(b * heads, heads), heads)
            for j in range(groups):
                om[here, j * LANES : (j + 1) * LANES] = jnp.where(masks[j], o[:, j * LANES : (j + 1) * LANES] * share, 0.0)

    pick = lax.broadcasted_iota(jnp.int32, (ROWS, seqs * heads), 1) // heads
    pick = jnp.where(pick == lax.broadcasted_iota(jnp.int32, (ROWS, seqs * heads), 0), 1.0, 0.0).astype(BF16)
    outs = nn(pick, om[...].astype(BF16))
    for j in range(groups):
        put_rows(so, j, outs[:, j * LANES : (j + 1) * LANES])

    @pl.loop(0, n_kv - 1)
    def _(i):
        k = kv_peer(i)
        send(ls.at[k % NX], rl.at[kv], R_LSE, kv=k)
        send(part(so, k % NX), part(ro, kv), R_ATT, kv=k)

    ro[kv] = so[xx]
    rl[kv] = ls[xx]

    @pl.when(owns)
    def _():
        got(O_A, roa, nz - 1)
        got(O_B, rob, nz - 1)

        def finished(n):
            a = functools.reduce(lambda t, z: t + roa[z, n, 0:ROWS, :].astype(F32), range(1, nz), roa[0, n, 0:ROWS, :].astype(F32))
            b = functools.reduce(lambda t, z: t + rob[z, n, 0:ROWS, :].astype(F32), range(1, nz), rob[0, n, 0:ROWS, :].astype(F32))
            return scale_mid * (a + half * b)

        k, v, f = [finished(n) for n in range(3)]
        qk = qf[xx] * k.astype(BF16).astype(F32)
        forget = jnp.minimum(f, 0.0) - jnp.log(1.0 + jnp.exp(-jnp.abs(f)))
        own0 = lane_sum(jnp.where(low, qk, 0.0)) * (HD**-0.5) - forget[:, 0:1]
        own1 = lane_sum(jnp.where(low, 0.0, qk)) * (HD**-0.5) - forget[:, HD : HD + 1]
        put_rows(ro, n_kv, v)
        rl[n_kv, 0:1, :] = flat(own0)
        rl[n_kv, 1:2, :] = flat(own1)
        to_all_z(rl, n_kv, Z_OWNL)
        to_all_z(ro, n_kv, Z_OWN)

    got(K_B, bb, n_kv - NX)
    for k in range(n_kv):
        mid[k] = rows_of(xb, k) + rows_of(bb, k) * half * gain(1, k)

    @pl.when(jnp.logical_not(owns))
    def _():
        wait(rsem.at[Z_OWNL], rl.at[n_kv])
        wait(rsem.at[Z_OWN], part(ro, n_kv))

    got(R_LSE, rl, n_kv - 1)
    n_src = n_kv + 1
    top = functools.reduce(jnp.maximum, [rl[s] for s in range(n_src)])
    raised = [jnp.exp(rl[s] - top) for s in range(n_src)]
    norm = 1.0 / functools.reduce(lambda a, b: a + b, raised)
    for s in range(n_src):
        wsq[2 * s : 2 * s + 2, :] = raised[s] * norm
    weights = wsq[...].T[0:ROWS]
    got(R_ATT, ro, n_kv - 1)
    joined = jnp.zeros((ROWS, LANES), F32)
    for s in range(n_src):
        joined = joined + jnp.where(low, weights[:, 2 * s : 2 * s + 1], weights[:, 2 * s + 1 : 2 * s + 2]) * rows_of(ro, s)
    attended = joined.astype(BF16)
    wait(rsem.at[X_WO], wo2.at[pl.ds(0, NX - 1)])
    for x in range(NX):
        put_rows(sm, x, nn(attended, wo2[x]))

    to_plane(sm, rm, P_MIX, lambda x: x)
    rm[me] = sm[xx]
    got(P_MIX, rm, n_plane - 1)
    put_rows(mb, kv, total_of(rm, range(n_plane)))

    to_all_kv(mb, K_MIX)
    for i in range(13, 16):
        loads[i].wait()

    got(K_MIX, mb, n_kv - 1)

    squares = jnp.zeros((ROWS, LANES), F32)
    for k in range(n_kv):
        v = rows_of(mb, k)
        squares = squares + v * v
    scale = lax.rsqrt(lane_sum(squares) / width + EPS)
    squares = jnp.zeros((ROWS, LANES), F32)
    for k in range(n_kv):
        v = mid[k] + rows_of(mb, k) * scale * gain(3, k)
        mid[k] = v
        squares = squares + v * v
    scale = lax.rsqrt(lane_sum(squares) / width + EPS)
    for k in range(n_kv):
        xn[:, k * LANES : (k + 1) * LANES] = (mid[k] * scale * gain(4, k)).astype(BF16)
    feed_forward(g2, l2, d2, pf2)
    to_kv_blocks(pf2, rf2, R_F2)
    got(R_F2, rf2, n_kv - 1)
    put_rows(tf2, tp, total_of(rf2, range(n_kv)))
    to_all_tp(tf2, T_F2)
    got(T_F2, tf2, n_tp - 1)
    bf = total_of(tf2, range(n_tp))

    stb[kv] = flat(lane_sum(bf * bf))
    to_all_kv(stb, K_STAT)
    got(K_STAT, stb, n_kv - 1)
    line = functools.reduce(lambda a, k: a + stb[k], range(1, n_kv), stb[0])
    scale = lax.rsqrt(upright(line) / width + EPS)
    final = (mid[kv] + 0.5 * (bf * scale * gains[5:6, pl.ds(col, LANES)])).astype(BF16)
    out_ref[...] = nt(place, final)[:, 0:seqs].astype(BF16)

    for stage, buf, n in (
        (T_TOK, ttok, n_tp - 1), (T_F2, tf2, n_tp - 1), (K_TOK, xb, n_kv - 1), (R_F1, pf, n_kv - 1), (P_F1, pb, n_plane - 1),
        (K_QA, qa, n_kv - 1), (K_QB, qb, n_kv - 1), (Z_ST, zst, nz - 1), (K_B, bb, n_kv - NX), (R_ATT, ro, n_kv - 1),
        (R_LSE, rl, n_kv - 1), (P_MIX, rm, n_plane - 1), (K_MIX, mb, n_kv - 1), (R_F2, pf2, n_kv - 1), (K_STAT, stb, n_kv - 1),
    ):
        gone(stage, buf, n)
    wait(ssem.at[X_W], wx.at[:, pl.ds(0, NX - 1)])
    wait(ssem.at[X_WO], wo2.at[pl.ds(0, NX - 1)])

    @pl.when(owns)
    def _():
        gone(Z_OWNL, rl, nz - 1)
        gone(Z_OWN, ro, nz - 1)

    @pl.when(jnp.logical_not(owns))
    def _():
        wait(ssem.at[O_A], oa.at[:, pl.ds(0, seqs)])
        wait(ssem.at[O_B], ob.at[:, pl.ds(0, seqs)])


def solution(mesh):
    n_kv, n_tp = mesh.shape["kv"], mesh.shape["tp"]
    axes = ("kv", "tp")

    def body(tokens, gains, g1, l1, d1, wq, wk, wv, wf, wo, g2, l2, d2, ck, cv, cd):
        seqs, own = tokens.shape
        width = own * n_kv * n_tp
        heads = cd.shape[1]
        groups = heads * HD // LANES
        nz, n_plane = n_kv // NX, NX * n_tp
        arrays = (tokens.T, gains, wq, wk, wv, wf.T, g1.T, l1.T, d1, ck, cd, cv, wo, g2.T, l2.T, d2)
        vm = pltpu.VMEM

        def blocks(*n):
            return vm((*n, TILE, LANES), BF16)

        scratch = [vm(a.shape, a.dtype) for a in arrays] + [
            blocks(n_tp),
            blocks(n_kv),
            vm((ROWS, width), BF16),
            vm((3, NX, LANES, LANES), BF16),
            vm((NX, LANES, LANES), BF16),
            blocks(n_kv),
            blocks(n_kv),
            blocks(n_plane),
            blocks(n_kv),
            blocks(n_kv),
            blocks(n_kv),
            blocks(3),
            blocks(3),
            blocks(nz, 3),
            blocks(nz, 3),
            vm((nz, 3, LANES), F32),
            vm((groups, ROWS, LANES), F32),
            vm((seqs, heads, cd.shape[2]), F32),
            vm((seqs, heads, cd.shape[2]), BF16),
            vm((seqs, heads, LANES), F32),
            vm((seqs * heads, heads * HD), F32),
            blocks(groups),
            vm((groups, 2, LANES), F32),
            blocks(n_kv + 1),
            vm((n_kv + 1, 2, LANES), F32),
            vm((LANES, LANES), F32),
            blocks(NX),
            blocks(n_plane),
            blocks(n_kv),
            vm((n_kv, ROWS, LANES), F32),
            blocks(n_kv),
            blocks(n_kv),
            blocks(n_tp),
            vm((n_kv, 1, LANES), F32),
            pltpu.SemaphoreType.DMA((len(arrays),)),
            pltpu.SemaphoreType.DMA((STAGES,)),
            pltpu.SemaphoreType.DMA((STAGES,)),
            pltpu.SemaphoreType.REGULAR((3,)),
        ]
        out = pl.pallas_call(
            functools.partial(kernel, n_kv, n_tp, seqs, width),
            out_shape=jax.ShapeDtypeStruct((own, seqs), BF16),
            in_specs=[pl.BlockSpec(memory_space=pl.ANY)] * len(arrays),
            out_specs=pl.BlockSpec(memory_space=pltpu.VMEM),
            scratch_shapes=scratch,
            compiler_params=pltpu.CompilerParams(
                collective_id=0, has_side_effects=True, vmem_limit_bytes=56 * 1024 * 1024
            ),
            name="layer",
        )(*arrays)
        return out.T

    placed = (
        P(None, axes), P(), P(None, axes), P(None, axes), P(axes, None), P("kv", "tp"), P("kv", "tp"), P("kv", "tp"),
        P(None, "tp"), P("tp", "kv"), P(None, axes), P(None, axes), P(axes, None), P(None, "kv", "tp"),
        P(None, "kv", "tp"), P(None, "tp", "kv"),
    )
    return jax.shard_map(body, mesh=mesh, in_specs=placed, out_specs=P(None, axes), check_vma=False)
```

time: 95.1 us -> 83.2 us (0.87)
  Pallas kernels: 93.7 us -> 81.7 us
    pallas_call x1, Pallas kernels: 93.7 us -> 81.7 us  [body(): pl.pallas_call(functools.partial(kernel, n_kv, n_tp, seqs, width), out_sh...]
where the time goes in v3:
time: 83.2 us; the launch traced here: 83 us
  Pallas kernels  81.7 us (98%)
  local copies, waits for them, and re-layouts  1.28 us (2%)
    pallas_call x1, Pallas kernels, body(): pl.pallas_call(functools.partial(kernel, n_kv, n_tp, seqs, width), out_sh...  81.7 us

profile of v3, /device:TPU:1, one launch (start us, length us, event | category | flops | bytes accessed | tf_op | source)
XLA Modules:
  0.0 83.0 jit_solution(18313643576233869424)
XLA Ops:
  0.0 81.7 %layer.1 = bf16[16,18]{1,0:T(8,128)(2,1)} custom-call(bf16[16,18]{1,0:T(8,128)(2,1)} %bitcast.13, f32[6,4096]{1,0:T(8,128)} %gains_h.1, bf16[128,512]{1,0:T(8,128)(2,1)} %wq_h.1, bf16[128,512]{1,0:T(8,128)(2,1)} %wk_h.1, bf16[128,512]{1,0:T(8,128)(2,1)} %wv_h.1, bf16[8,4096]{1,0:T(8,128)(2,1)} %bitcast.11, bf16[44,4096]{1,0:T(8,128)(2,1)} %bitcast.7, ...), custom_call_target="tpu_custom_call" | custom-call | tf_op jit(solution)/shard_map/layer/pallas_call | solution.py:514
  81.7 1.3 %copy.18 = bf16[18,16]{0,1:T(8,128)(2,1)} copy(bf16[18,16]{0,1:T(8,128)(2,1)} %bitcast.12) | data formatting | bytes 1152

commit v4 on v3

--- a/solution.py
+++ b/solution.py
@@ -15,8 +15,8 @@
 ROWS = 24
 TILE = 32
 NX = 4
-STAGES = 21
-(T_TOK, K_TOK, X_W, X_WO, R_F1, P_F1, K_QA, K_QB, O_A, O_B, Z_ST, Z_OWN, Z_OWNL, K_B, R_ATT, R_LSE, P_MIX, K_MIX,
+STAGES = 22
+(T_TOK, K_TOK, X_Q, X_W, X_WO, R_F1, P_F1, K_QA, K_QB, O_A, O_B, Z_ST, Z_OWN, Z_OWNL, K_B, R_ATT, R_LSE, P_MIX, K_MIX,
  R_F2, T_F2, K_STAT) = range(STAGES)
 
 
@@ -57,8 +57,8 @@
     n_kv, n_tp, seqs, width,
     tok_h, gains_h, wq_h, wk_h, wv_h, wf_h, g1_h, l1_h, d1_h, ck_h, cd_h, cv_h, wo_h, g2_h, l2_h, d2_h,
     out_ref,
-    tok, gains, wq, wk, wv, wf, g1, l1, d1, ck, cd, cv, wo, g2, l2, d2,
-    ttok, xb, xn, wx, wo2, pf, rf, pb, bb, qa, qb, oa, ob, roa, rob, zst, qf, sc, wt, si, om, so, ls, ro, rl, wsq,
+    tok, gains, wk, wv, wf, g1, l1, d1, ck, cd, cv, wo, g2, l2, d2,
+    ttok, xb, xn, wqf, wx, wo2, pf, rf, pb, bb, qa, qb, oa, ob, roa, rob, zst, qf, sc, wt, si, om, so, ls, ro, rl, wsq,
     sm, rm, mb, mid, pf2, rf2, tf2, stb,
     load_sem, ssem, rsem, hello,
 ):
@@ -77,7 +77,7 @@
     loads = [
         pltpu.make_async_copy(h, v, load_sem.at[i])
         for i, (h, v) in enumerate(
-            [(tok_h, tok), (gains_h, gains), (wq_h, wq), (wk_h, wk), (wv_h, wv), (wf_h, wf), (g1_h, g1), (l1_h, l1),
+            [(tok_h, tok), (gains_h, gains), (wq_h, wqf.at[xx]), (wk_h, wk), (wv_h, wv), (wf_h, wf), (g1_h, g1), (l1_h, l1),
              (d1_h, d1), (ck_h, ck), (cd_h, cd), (cv_h, cv), (wo_h, wo), (g2_h, g2), (l2_h, l2), (d2_h, d2)]
         )
     ]
@@ -87,20 +87,37 @@
     def ordered(i, n):
         return (n // 2 + ((i + 1) // 2) * (1 - 2 * (i % 2)) + n) % n
 
+    def shift(i, d, n):
+        return lax.rem(i + d, n)
+
     def kv_at(dz, dx):
-        return ((zz + dz + nz) % nz) * NX + (xx + dx) % NX
-
-    def kv_peer(i):
-        return kv_at(ordered(i // NX, nz), ordered(i % NX, NX))
-
-    def tp_peer(i):
-        return (tp + 1 + i) % n_tp
-
-    def plane_peer(i):
-        return (xx + ordered(i // n_tp, NX)) % NX, (tp + 1 + i % n_tp) % n_tp
+        return shift(zz, dz % nz, nz) * NX + shift(xx, dx, NX)
+
+    x_of = [shift(xx, ordered(i, NX), NX) for i in range(NX)]
 
     def at(x):
         return zz * NX + x
+
+    def each_kv(visit, same_z=True):
+        @pl.loop(0, nz - 1)
+        def _(i):
+            first = shift(zz, ordered(i, nz), nz) * NX
+            for x in x_of:
+                visit(first + x, x)
+
+        if same_z:
+            for x in x_of[:-1]:
+                visit(at(x), x)
+
+    def each_plane(visit):
+        @pl.loop(0, n_tp - 1)
+        def _(i):
+            t = shift(tp, ordered(i, n_tp), n_tp)
+            for x in x_of:
+                visit(x, t)
+
+        for x in x_of[:-1]:
+            visit(x, tp)
 
     z_own = (2 * xx + tp) % nz
     owns = zz == z_own
@@ -127,32 +144,26 @@
     def gone(stage, buf, n):
         wait(ssem.at[stage], part(buf, pl.ds(0, n)))
 
-    def to_all_kv(buf, stage, count=n_kv - 1):
-        @pl.loop(0, count)
-        def _(i):
-            send(part(buf, kv), part(buf, kv), stage, kv=kv_peer(i))
+    def to_all_kv(buf, stage, same_z=True):
+        each_kv(lambda k, x: send(part(buf, kv), part(buf, kv), stage, kv=k), same_z)
 
     def to_all_tp(buf, stage):
         @pl.loop(0, n_tp - 1)
         def _(i):
-            send(part(buf, tp), part(buf, tp), stage, tp=tp_peer(i))
+            send(part(buf, tp), part(buf, tp), stage, tp=shift(tp, ordered(i, n_tp), n_tp))
 
     def to_all_z(buf, slot, stage):
         @pl.loop(0, nz - 1)
         def _(i):
-            send(part(buf, slot), part(buf, slot), stage, kv=kv_at(ordered(i, nz), 0))
+            send(part(buf, slot), part(buf, slot), stage, kv=shift(zz, ordered(i, nz), nz) * NX + xx)
 
     def to_kv_blocks(src, dst, stage):
-        @pl.loop(0, n_kv - 1)
-        def _(i):
-            k = kv_peer(i)
-            send(part(src, k), part(dst, kv), stage, kv=k)
-
+        each_kv(lambda k, x: send(part(src, k), part(dst, kv), stage, kv=k))
         dst[kv] = src[kv]
 
     barrier = pltpu.get_barrier_semaphore()
     for i in range(n_tp - 1):
-        pl.semaphore_signal(barrier, inc=1, device_id={"tp": tp_peer(i)}, device_id_type=MESH)
+        pl.semaphore_signal(barrier, inc=1, device_id={"tp": shift(tp, i + 1, n_tp)}, device_id_type=MESH)
     for dz, dx in [(0, d) for d in range(1, NX)] + [(1, 0), (-1, 0)]:
         pl.semaphore_signal(barrier, inc=1, device_id={"kv": kv_at(dz, dx)}, device_id_type=MESH)
 
@@ -166,22 +177,31 @@
 
     pl.semaphore_wait(barrier, n_tp - 1 + NX - 1 + 2)
 
+    def hear(n, step):
+        for dz in (step, -step):
+            pl.semaphore_signal(hello.at[n], inc=1, device_id={"kv": kv_at(dz, 0)}, device_id_type=MESH)
+        if n != 1:
+            pl.semaphore_wait(hello.at[n], 2)
+
     to_all_tp(ttok, T_TOK)
-    for i in range(2, 5):
+    hear(0, 1)
+    hear(1, 2)
+    for i in range(3, 5):
         loads[i].wait()
     for d in range(1, NX):
-        j = (xx + d) % NX
-        for m, w in enumerate((wq, wk, wv)):
+        j = shift(xx, d, NX)
+        for m, w in enumerate((wk, wv)):
             send(w.at[:, pl.ds(pl.multiple_of(j * LANES, LANES), LANES)], wx.at[m, xx], X_W, kv=at(j))
-    for m, w in enumerate((wq, wk, wv)):
+    pl.semaphore_wait(hello.at[1], 2)
+    hear(2, 1)
+    for m, w in enumerate((wk, wv)):
         wx[m, xx] = w[:, pl.ds(xcol, LANES)]
-    for n, step in enumerate((1, 2, 1)):
-        for dz in (step, -step):
-            pl.semaphore_signal(hello.at[n], inc=1, device_id={"kv": kv_at(dz, 0)}, device_id_type=MESH)
-        pl.semaphore_wait(hello.at[n], 2)
     got(T_TOK, ttok, n_tp - 1)
     put_rows(xb, kv, total_of(ttok, range(n_tp)))
     to_all_kv(xb, K_TOK)
+    loads[2].wait()
+    for x in x_of[:-1]:
+        send(wqf.at[xx], wqf.at[xx], X_Q, kv=at(x))
 
     def gain(i, k):
         return gains[i : i + 1, k * LANES : (k + 1) * LANES]
@@ -224,14 +244,17 @@
 
     loads[5].wait()
     wait(rsem.at[X_W], wx.at[:, pl.ds(0, NX - 1)])
+    got(X_Q, wqf, NX - 1)
     tz = jnp.concatenate([rows_of(xb, at(x)) for x in range(NX)], axis=1)
     lane_f = lax.broadcasted_iota(jnp.int32, (ROWS, heads), 1)
 
     def projections(x, q_out, o_out):
-        q, k, v = [nn(x, wx[m].reshape(zwide, LANES)) for m in range(3)]
+        q = nn(x, wqf[...].reshape(zwide, groups * LANES))
+        k, v = [nn(x, wx[m].reshape(zwide, LANES)) for m in range(2)]
         f = nt(x, wf[:, pl.ds(zcol, zwide)])
         f0, f1 = [lane_sum(jnp.where(lane_f == 2 * xx + g, f, 0.0)) for g in range(2)]
-        put_rows(q_out, kv, q)
+        for j in range(groups):
+            q_out[zz, j, 0:ROWS, :] = q[:, j * LANES : (j + 1) * LANES].astype(BF16)
         put_rows(o_out, 0, k)
         put_rows(o_out, 1, v)
         put_rows(o_out, 2, jnp.where(low, f0, f1))
@@ -253,13 +276,10 @@
     put_rows(pb, me, total_of(rf, range(n_kv)))
 
     def to_plane(src, dst, stage, pick):
-        @pl.loop(0, n_plane - 1)
-        def _(i):
-            x, t = plane_peer(i)
-            send(part(src, pick(x)), part(dst, me), stage, kv=at(x), tp=t)
+        each_plane(lambda x, t: send(part(src, pick(x)), part(dst, me), stage, kv=at(x), tp=t))
 
     to_plane(pb, pb, P_F1, lambda x: me)
-    to_all_kv(qa, K_QA)
+    to_all_z(qa, zz, K_QA)
     to_owner(oa, roa, O_A)
 
     got(P_F1, pb, n_plane - 1)
@@ -268,28 +288,27 @@
     bz = jnp.concatenate([rows_of(bb, at(x)) for x in range(NX)], axis=1)
     u = bz * zgain(1)
     projections((u * zgain(2)).astype(BF16), qb, ob)
-    to_all_kv(qb, K_QB)
+    to_all_z(qb, zz, K_QB)
     for n, stat in enumerate((bz * bz, tz * u, u * u)):
         zst[zz, n : n + 1, :] = flat(lane_sum(stat))
     to_all_z(zst, zz, Z_ST)
     to_owner(ob, rob, O_B)
 
-    got(K_QA, qa, n_kv - 1)
+    got(K_QA, qa, nz - 1)
     got(Z_ST, zst, nz - 1)
     stats = functools.reduce(lambda a, z: a + zst[z], range(1, nz), zst[0])
     s_bb, s_tu, s_uu = [upright(stats[n : n + 1]) for n in range(3)]
     r1 = lax.rsqrt(s_bb / width + EPS)
     half = 0.5 * r1
     scale_mid = lax.rsqrt((s_tt + r1 * s_tu + half * half * s_uu) / width + EPS)
-    got(K_QB, qb, n_kv - 1)
+    got(K_QB, qb, nz - 1)
     for j in range(groups):
-        slots = range(j, n_kv, NX)
-        qf[j] = (scale_mid * (total_of(qa, slots) + half * total_of(qb, slots))).astype(BF16).astype(F32)
-
-    to_all_kv(bb, K_B, n_kv - NX)
+        a, b = [functools.reduce(lambda t, more: t + more, [p[z, j, 0:ROWS, :].astype(F32) for z in range(nz)]) for p in (qa, qb)]
+        qf[j] = (scale_mid * (a + half * b)).astype(BF16).astype(F32)
+
     loads[12].wait()
     for d in range(1, NX):
-        j = (xx + d) % NX
+        j = shift(xx, d, NX)
         send(wo.at[pl.ds(pl.multiple_of(j * LANES, LANES), LANES), :], wo2.at[xx], X_WO, kv=at(j))
     wo2[xx] = wo[pl.ds(xcol, LANES), :]
     for i in range(9, 12):
@@ -297,7 +316,7 @@
     head_i = lax.broadcasted_iota(jnp.int32, (heads, LANES), 0)
     lane_h = lax.broadcasted_iota(jnp.int32, (heads, LANES), 1)
     masks = [head_i == 2 * j + lane_h // HD for j in range(groups)]
-    batch = 6
+    batch = 18
 
     @pl.loop(0, seqs, step=batch)
     def _(first):
@@ -339,12 +358,11 @@
     for j in range(groups):
         put_rows(so, j, outs[:, j * LANES : (j + 1) * LANES])
 
-    @pl.loop(0, n_kv - 1)
-    def _(i):
-        k = kv_peer(i)
-        send(ls.at[k % NX], rl.at[kv], R_LSE, kv=k)
-        send(part(so, k % NX), part(ro, kv), R_ATT, kv=k)
-
+    def deliver(k, x):
+        send(ls.at[x], rl.at[kv], R_LSE, kv=k)
+        send(part(so, x), part(ro, kv), R_ATT, kv=k)
+
+    each_kv(deliver)
     ro[kv] = so[xx]
     rl[kv] = ls[xx]
 
@@ -368,10 +386,6 @@
         rl[n_kv, 1:2, :] = flat(own1)
         to_all_z(rl, n_kv, Z_OWNL)
         to_all_z(ro, n_kv, Z_OWN)
-
-    got(K_B, bb, n_kv - NX)
-    for k in range(n_kv):
-        mid[k] = rows_of(xb, k) + rows_of(bb, k) * half * gain(1, k)
 
     @pl.when(jnp.logical_not(owns))
     def _():
@@ -397,12 +411,17 @@
 
     to_plane(sm, rm, P_MIX, lambda x: x)
     rm[me] = sm[xx]
+    to_all_kv(bb, K_B, False)
     got(P_MIX, rm, n_plane - 1)
     put_rows(mb, kv, total_of(rm, range(n_plane)))
 
     to_all_kv(mb, K_MIX)
     for i in range(13, 16):
         loads[i].wait()
+
+    got(K_B, bb, n_kv - NX)
+    for k in range(n_kv):
+        mid[k] = rows_of(xb, k) + rows_of(bb, k) * half * gain(1, k)
 
     got(K_MIX, mb, n_kv - 1)
 
@@ -437,7 +456,7 @@
 
     for stage, buf, n in (
         (T_TOK, ttok, n_tp - 1), (T_F2, tf2, n_tp - 1), (K_TOK, xb, n_kv - 1), (R_F1, pf, n_kv - 1), (P_F1, pb, n_plane - 1),
-        (K_QA, qa, n_kv - 1), (K_QB, qb, n_kv - 1), (Z_ST, zst, nz - 1), (K_B, bb, n_kv - NX), (R_ATT, ro, n_kv - 1),
+        (K_QA, qa, nz - 1), (K_QB, qb, nz - 1), (X_Q, wqf, NX - 1), (Z_ST, zst, nz - 1), (K_B, bb, n_kv - NX), (R_ATT, ro, n_kv - 1),
         (R_LSE, rl, n_kv - 1), (P_MIX, rm, n_plane - 1), (K_MIX, mb, n_kv - 1), (R_F2, pf2, n_kv - 1), (K_STAT, stb, n_kv - 1),
     ):
         gone(stage, buf, n)
@@ -466,23 +485,25 @@
         groups = heads * HD // LANES
         nz, n_plane = n_kv // NX, NX * n_tp
         arrays = (tokens.T, gains, wq, wk, wv, wf.T, g1.T, l1.T, d1, ck, cd, cv, wo, g2.T, l2.T, d2)
+        arrays = tuple(pltpu.with_memory_space_constraint(a, pltpu.HBM) for a in arrays)
         vm = pltpu.VMEM
 
         def blocks(*n):
             return vm((*n, TILE, LANES), BF16)
 
-        scratch = [vm(a.shape, a.dtype) for a in arrays] + [
+        scratch = [vm(a.shape, a.dtype) for i, a in enumerate(arrays) if i != 2] + [
             blocks(n_tp),
             blocks(n_kv),
             vm((ROWS, width), BF16),
-            vm((3, NX, LANES, LANES), BF16),
+            vm((NX, LANES, groups * LANES), BF16),
+            vm((2, NX, LANES, LANES), BF16),
             vm((NX, LANES, LANES), BF16),
             blocks(n_kv),
             blocks(n_kv),
             blocks(n_plane),
             blocks(n_kv),
-            blocks(n_kv),
-            blocks(n_kv),
+            blocks(nz, groups),
+            blocks(nz, groups),
             blocks(3),
             blocks(3),
             blocks(nz, 3),
@@ -518,7 +539,7 @@
             out_specs=pl.BlockSpec(memory_space=pltpu.VMEM),
             scratch_shapes=scratch,
             compiler_params=pltpu.CompilerParams(
-                collective_id=0, has_side_effects=True, vmem_limit_bytes=56 * 1024 * 1024
+                collective_id=0, has_side_effects=True, vmem_limit_bytes=26 * 1024 * 1024
             ),
             name="layer",
         )(*arrays)

time: 83.2 us -> 77.9 us (0.936)
  Pallas kernels: 81.7 us -> 77.1 us
    pallas_call x1, Pallas kernels: 81.7 us -> 77.1 us  [body(): pl.pallas_call(functools.partial(kernel, n_kv, n_tp, seqs, width), out_sh...]
where the time goes in v4:
time: 77.9 us; the launch traced here: 77.7 us
  Pallas kernels  77.1 us (99%)
    pallas_call x1, Pallas kernels, body(): pl.pallas_call(functools.partial(kernel, n_kv, n_tp, seqs, width), out_sh...  77.1 us

profile of v4, /device:TPU:1, one launch (start us, length us, event | category | flops | bytes accessed | tf_op | source)
XLA Modules:
  0.0 77.7 jit_solution(13386428878714087241)
XLA Ops:
  0.0 77.1 %layer.1 = bf16[16,18]{1,0:T(8,128)(2,1)S(1)} custom-call(bf16[16,18]{1,0:T(8,128)(2,1)} %bitcast.13, f32[6,4096]{1,0:T(8,128)} %gains_h.1, bf16[128,512]{1,0:T(8,128)(2,1)} %wq_h.1, bf16[128,512]{1,0:T(8,128)(2,1)} %wk_h.1, bf16[128,512]{1,0:T(8,128)(2,1)} %wv_h.1, bf16[8,4096]{1,0:T(8,128)(2,1)} %bitcast.12, bf16[44,4096]{1,0:T(8,128)(2,1)} %bitcast.8, ...), custom_call_target="tpu_custom_call" | custom-call | tf_op jit(solution)/shard_map/layer/pallas_call | solution.py:535
  77.1 0.6 copy.18

commit v5 on v4

--- a/solution.py
+++ b/solution.py
@@ -58,7 +58,7 @@
     tok_h, gains_h, wq_h, wk_h, wv_h, wf_h, g1_h, l1_h, d1_h, ck_h, cd_h, cv_h, wo_h, g2_h, l2_h, d2_h,
     out_ref,
     tok, gains, wk, wv, wf, g1, l1, d1, ck, cd, cv, wo, g2, l2, d2,
-    ttok, xb, xn, wqf, wx, wo2, pf, rf, pb, bb, qa, qb, oa, ob, roa, rob, zst, qf, sc, wt, si, om, so, ls, ro, rl, wsq,
+    ckt, ttok, xb, wqf, wx, wo2, pf, rf, pb, bb, qa, qb, oa, ob, roa, rob, zst, qf, sc, wt, si, om, so, ls, ro, rl, wsq, wexp,
     sm, rm, mb, mid, pf2, rf2, tf2, stb,
     load_sem, ssem, rsem, hello,
 ):
@@ -209,9 +209,22 @@
     def zgain(i):
         return gains[i : i + 1, pl.ds(zcol, zwide)]
 
-    def feed_forward(gate_w, lift_w, down_w, part_out):
-        x = xn[...]
-        act = (silu(nt(x, gate_w[...])) * nt(x, lift_w[...])).astype(BF16)
+    def products(block, gain_row, gate_w, lift_w):
+        squares, gate, lift = [jnp.zeros((ROWS, n), F32) for n in (LANES, gate_w.shape[0], lift_w.shape[0])]
+        for c in range(0, n_kv, 4):
+            xs = []
+            for k in range(c, c + 4):
+                v = block(k)
+                squares = squares + v * v
+                xs.append((v * gain(gain_row, k)).astype(BF16))
+            x = jnp.concatenate(xs, axis=1)
+            here = slice(c * LANES, (c + 4) * LANES)
+            gate = gate + nt(x, gate_w[:, here])
+            lift = lift + nt(x, lift_w[:, here])
+        return lane_sum(squares), gate, lift
+
+    def feed_forward(scale, gate, lift, down_w, part_out):
+        act = (silu(gate * scale) * (lift * scale)).astype(BF16)
         for c in range(0, n_kv, 4):
             some = nn(act, down_w[:, c * LANES : (c + 4) * LANES])
             for j in range(4):
@@ -229,18 +242,17 @@
 
     loads[1].wait()
     got(K_TOK, xb, n_kv - 1)
-    squares = jnp.zeros((ROWS, LANES), F32)
-    for k in range(n_kv):
-        v = rows_of(xb, k)
-        squares = squares + v * v
-    s_tt = lane_sum(squares)
-    scale = lax.rsqrt(s_tt / width + EPS)
-    for k in range(n_kv):
-        xn[:, k * LANES : (k + 1) * LANES] = (rows_of(xb, k) * scale * gain(0, k)).astype(BF16)
     for i in range(6, 9):
         loads[i].wait()
-    feed_forward(g1, l1, d1, pf)
+    s_tt, gate, lift = products(lambda k: rows_of(xb, k), 0, g1, l1)
+    feed_forward(lax.rsqrt(s_tt / width + EPS), gate, lift, d1, pf)
     to_kv_blocks(pf, rf, R_F1)
+
+    loads[9].wait()
+
+    @pl.loop(0, seqs)
+    def _(b):
+        ckt[b] = ck[b].T
 
     loads[5].wait()
     wait(rsem.at[X_W], wx.at[:, pl.ds(0, NX - 1)])
@@ -248,15 +260,16 @@
     tz = jnp.concatenate([rows_of(xb, at(x)) for x in range(NX)], axis=1)
     lane_f = lax.broadcasted_iota(jnp.int32, (ROWS, heads), 1)
 
-    def projections(x, q_out, o_out):
+    def query_part(x, q_out):
         q = nn(x, wqf[...].reshape(zwide, groups * LANES))
-        k, v = [nn(x, wx[m].reshape(zwide, LANES)) for m in range(2)]
+        for j in range(groups):
+            q_out[zz, j, 0:ROWS, :] = q[:, j * LANES : (j + 1) * LANES].astype(BF16)
+
+    def other_parts(x, o_out):
+        for m in range(2):
+            put_rows(o_out, m, nn(x, wx[m].reshape(zwide, LANES)))
         f = nt(x, wf[:, pl.ds(zcol, zwide)])
         f0, f1 = [lane_sum(jnp.where(lane_f == 2 * xx + g, f, 0.0)) for g in range(2)]
-        for j in range(groups):
-            q_out[zz, j, 0:ROWS, :] = q[:, j * LANES : (j + 1) * LANES].astype(BF16)
-        put_rows(o_out, 0, k)
-        put_rows(o_out, 1, v)
         put_rows(o_out, 2, jnp.where(low, f0, f1))
 
     def to_owner(src, dst, stage):
@@ -270,7 +283,9 @@
         def _():
             dst[zz] = src[...]
 
-    projections((tz * zgain(2)).astype(BF16), qa, oa)
+    shared = (tz * zgain(2)).astype(BF16)
+    query_part(shared, qa)
+    other_parts(shared, oa)
 
     got(R_F1, rf, n_kv - 1)
     put_rows(pb, me, total_of(rf, range(n_kv)))
@@ -287,11 +302,13 @@
         put_rows(bb, at(x), total_of(pb, range(x * n_tp, (x + 1) * n_tp)))
     bz = jnp.concatenate([rows_of(bb, at(x)) for x in range(NX)], axis=1)
     u = bz * zgain(1)
-    projections((u * zgain(2)).astype(BF16), qb, ob)
+    shared = (u * zgain(2)).astype(BF16)
+    query_part(shared, qb)
     to_all_z(qb, zz, K_QB)
     for n, stat in enumerate((bz * bz, tz * u, u * u)):
         zst[zz, n : n + 1, :] = flat(lane_sum(stat))
     to_all_z(zst, zz, Z_ST)
+    other_parts(shared, ob)
     to_owner(ob, rob, O_B)
 
     got(K_QA, qa, nz - 1)
@@ -301,32 +318,29 @@
     r1 = lax.rsqrt(s_bb / width + EPS)
     half = 0.5 * r1
     scale_mid = lax.rsqrt((s_tt + r1 * s_tu + half * half * s_uu) / width + EPS)
+
+    def z_sum(buf, j):
+        return functools.reduce(lambda a, b: a + b, [buf[z, j, 0:ROWS, :].astype(F32) for z in range(nz)])
+
+    from_tokens = [z_sum(qa, j) for j in range(groups)]
     got(K_QB, qb, nz - 1)
     for j in range(groups):
-        a, b = [functools.reduce(lambda t, more: t + more, [p[z, j, 0:ROWS, :].astype(F32) for z in range(nz)]) for p in (qa, qb)]
-        qf[j] = (scale_mid * (a + half * b)).astype(BF16).astype(F32)
+        qf[j] = (scale_mid * (from_tokens[j] + half * z_sum(qb, j))).astype(BF16).astype(F32)
 
     loads[12].wait()
     for d in range(1, NX):
         j = shift(xx, d, NX)
         send(wo.at[pl.ds(pl.multiple_of(j * LANES, LANES), LANES), :], wo2.at[xx], X_WO, kv=at(j))
     wo2[xx] = wo[pl.ds(xcol, LANES), :]
-    for i in range(9, 12):
+    for i in range(10, 12):
         loads[i].wait()
     head_i = lax.broadcasted_iota(jnp.int32, (heads, LANES), 0)
     lane_h = lax.broadcasted_iota(jnp.int32, (heads, LANES), 1)
     masks = [head_i == 2 * j + lane_h // HD for j in range(groups)]
-    batch = 18
-
-    @pl.loop(0, seqs, step=batch)
-    def _(first):
-        for i in range(batch):
-            b = first + i
-            rows = [
-                jnp.where(masks[j], jnp.broadcast_to(qf[j, pl.ds(b, 1), :], (heads, LANES)), 0.0) for j in range(groups)
-            ]
-            query = jnp.concatenate(rows, axis=1).astype(BF16)
-            sc[b] = nt(query, ck[b]) * (HD**-0.5) + cd[b]
+    for b in range(seqs):
+        rows = [jnp.where(masks[j], jnp.broadcast_to(qf[j, b : b + 1, :], (heads, LANES)), 0.0) for j in range(groups)]
+        query = jnp.concatenate(rows, axis=1).astype(BF16)
+        sc[b] = nn(query, ckt[b]) * (HD**-0.5) + cd[b]
 
     score = sc[...]
     peak = jnp.max(score, axis=2, keepdims=True)
@@ -342,15 +356,18 @@
     for j in range(groups):
         ls[j] = lines[2 * j : 2 * j + 2]
 
-    @pl.loop(0, seqs, step=batch)
-    def _(first):
-        for i in range(batch):
-            b = first + i
-            o = nn(wt[b], cv[b])
-            share = si[b]
-            here = pl.ds(pl.multiple_of(b * heads, heads), heads)
-            for j in range(groups):
-                om[here, j * LANES : (j + 1) * LANES] = jnp.where(masks[j], o[:, j * LANES : (j + 1) * LANES] * share, 0.0)
+    for i in range(n_kv - 1):
+        first, x = shift(zz, ordered(i // NX, nz), nz) * NX, x_of[i % NX]
+        send(ls.at[x], rl.at[kv], R_LSE, kv=first + x)
+    rl[kv] = ls[xx]
+
+    for b in range(seqs):
+        o = nn(wt[b], cv[b])
+        share = si[b]
+        for j in range(groups):
+            om[b * heads : (b + 1) * heads, j * LANES : (j + 1) * LANES] = jnp.where(
+                masks[j], o[:, j * LANES : (j + 1) * LANES] * share, 0.0
+            )
 
     pick = lax.broadcasted_iota(jnp.int32, (ROWS, seqs * heads), 1) // heads
     pick = jnp.where(pick == lax.broadcasted_iota(jnp.int32, (ROWS, seqs * heads), 0), 1.0, 0.0).astype(BF16)
@@ -358,13 +375,8 @@
     for j in range(groups):
         put_rows(so, j, outs[:, j * LANES : (j + 1) * LANES])
 
-    def deliver(k, x):
-        send(ls.at[x], rl.at[kv], R_LSE, kv=k)
-        send(part(so, x), part(ro, kv), R_ATT, kv=k)
-
-    each_kv(deliver)
+    each_kv(lambda k, x: send(part(so, x), part(ro, kv), R_ATT, kv=k))
     ro[kv] = so[xx]
-    rl[kv] = ls[xx]
 
     @pl.when(owns)
     def _():
@@ -390,7 +402,6 @@
     @pl.when(jnp.logical_not(owns))
     def _():
         wait(rsem.at[Z_OWNL], rl.at[n_kv])
-        wait(rsem.at[Z_OWN], part(ro, n_kv))
 
     got(R_LSE, rl, n_kv - 1)
     n_src = n_kv + 1
@@ -400,10 +411,17 @@
     for s in range(n_src):
         wsq[2 * s : 2 * s + 2, :] = raised[s] * norm
     weights = wsq[...].T[0:ROWS]
+    for s in range(n_src):
+        wexp[s] = jnp.where(low, weights[:, 2 * s : 2 * s + 1], weights[:, 2 * s + 1 : 2 * s + 2])
+
+    @pl.when(jnp.logical_not(owns))
+    def _():
+        wait(rsem.at[Z_OWN], part(ro, n_kv))
+
     got(R_ATT, ro, n_kv - 1)
     joined = jnp.zeros((ROWS, LANES), F32)
     for s in range(n_src):
-        joined = joined + jnp.where(low, weights[:, 2 * s : 2 * s + 1], weights[:, 2 * s + 1 : 2 * s + 2]) * rows_of(ro, s)
+        joined = joined + wexp[s] * rows_of(ro, s)
     attended = joined.astype(BF16)
     wait(rsem.at[X_WO], wo2.at[pl.ds(0, NX - 1)])
     for x in range(NX):
@@ -430,15 +448,13 @@
         v = rows_of(mb, k)
         squares = squares + v * v
     scale = lax.rsqrt(lane_sum(squares) / width + EPS)
-    squares = jnp.zeros((ROWS, LANES), F32)
-    for k in range(n_kv):
-        v = mid[k] + rows_of(mb, k) * scale * gain(3, k)
-        mid[k] = v
-        squares = squares + v * v
-    scale = lax.rsqrt(lane_sum(squares) / width + EPS)
-    for k in range(n_kv):
-        xn[:, k * LANES : (k + 1) * LANES] = (mid[k] * scale * gain(4, k)).astype(BF16)
-    feed_forward(g2, l2, d2, pf2)
+
+    def after(k):
+        mid[k] = mid[k] + rows_of(mb, k) * scale * gain(3, k)
+        return mid[k]
+
+    s_aa, gate, lift = products(after, 4, g2, l2)
+    feed_forward(lax.rsqrt(s_aa / width + EPS), gate, lift, d2, pf2)
     to_kv_blocks(pf2, rf2, R_F2)
     got(R_F2, rf2, n_kv - 1)
     put_rows(tf2, tp, total_of(rf2, range(n_kv)))
@@ -492,9 +508,9 @@
             return vm((*n, TILE, LANES), BF16)
 
         scratch = [vm(a.shape, a.dtype) for i, a in enumerate(arrays) if i != 2] + [
+            vm((seqs, heads * HD, cd.shape[2]), BF16),
             blocks(n_tp),
             blocks(n_kv),
-            vm((ROWS, width), BF16),
             vm((NX, LANES, groups * LANES), BF16),
             vm((2, NX, LANES, LANES), BF16),
             vm((NX, LANES, LANES), BF16),
@@ -519,6 +535,7 @@
             blocks(n_kv + 1),
             vm((n_kv + 1, 2, LANES), F32),
             vm((LANES, LANES), F32),
+            vm((n_kv + 1, ROWS, LANES), F32),
             blocks(NX),
             blocks(n_plane),
             blocks(n_kv),
@@ -539,7 +556,7 @@
             out_specs=pl.BlockSpec(memory_space=pltpu.VMEM),
             scratch_shapes=scratch,
             compiler_params=pltpu.CompilerParams(
-                collective_id=0, has_side_effects=True, vmem_limit_bytes=26 * 1024 * 1024
+                collective_id=0, has_side_effects=True, vmem_limit_bytes=36 * 1024 * 1024
             ),
             name="layer",
         )(*arrays)

time: 77.9 us -> 76.9 us (0.987)
  Pallas kernels: 77.1 us -> 76.2 us
    pallas_call x1, Pallas kernels: 77.1 us -> 76.2 us  [body(): pl.pallas_call(functools.partial(kernel, n_kv, n_tp, seqs, width), out_sh...]
where the time goes in v5:
time: 76.9 us; the launch traced here: 76.8 us
  Pallas kernels  76.2 us (99%)
    pallas_call x1, Pallas kernels, body(): pl.pallas_call(functools.partial(kernel, n_kv, n_tp, seqs, width), out_sh...  76.2 us

profile of v5, /device:TPU:1, one launch (start us, length us, event | category | flops | bytes accessed | tf_op | source)
XLA Modules:
  0.0 76.8 jit_solution(445936691171696403)
XLA Ops:
  0.0 76.2 %layer.1 = bf16[16,18]{1,0:T(8,128)(2,1)S(1)} custom-call(bf16[16,18]{1,0:T(8,128)(2,1)} %bitcast.13, f32[6,4096]{1,0:T(8,128)} %gains_h.1, bf16[128,512]{1,0:T(8,128)(2,1)} %wq_h.1, bf16[128,512]{1,0:T(8,128)(2,1)} %wk_h.1, bf16[128,512]{1,0:T(8,128)(2,1)} %wv_h.1, bf16[8,4096]{1,0:T(8,128)(2,1)} %bitcast.12, bf16[44,4096]{1,0:T(8,128)(2,1)} %bitcast.8, ...), custom_call_target="tpu_custom_call" | custom-call | tf_op jit(solution)/shard_map/layer/pallas_call | solution.py:552
  76.2 0.6 copy.18

commit v6 on v5

--- a/solution.py
+++ b/solution.py
@@ -304,10 +304,10 @@
     u = bz * zgain(1)
     shared = (u * zgain(2)).astype(BF16)
     query_part(shared, qb)
-    to_all_z(qb, zz, K_QB)
     for n, stat in enumerate((bz * bz, tz * u, u * u)):
         zst[zz, n : n + 1, :] = flat(lane_sum(stat))
     to_all_z(zst, zz, Z_ST)
+    to_all_z(qb, zz, K_QB)
     other_parts(shared, ob)
     to_owner(ob, rob, O_B)
 
@@ -317,7 +317,7 @@
     s_bb, s_tu, s_uu = [upright(stats[n : n + 1]) for n in range(3)]
     r1 = lax.rsqrt(s_bb / width + EPS)
     half = 0.5 * r1
-    scale_mid = lax.rsqrt((s_tt + r1 * s_tu + half * half * s_uu) / width + EPS)
+    scale_mid = lax.rsqrt(jnp.maximum(s_tt + r1 * s_tu + half * half * s_uu, 0.0) / width + EPS)
 
     def z_sum(buf, j):
         return functools.reduce(lambda a, b: a + b, [buf[z, j, 0:ROWS, :].astype(F32) for z in range(nz)])

time: 76.9 us -> 76.1 us (0.990)
  Pallas kernels: 76.2 us -> 75.3 us
    pallas_call x1, Pallas kernels: 76.2 us -> 75.3 us  [body(): pl.pallas_call(functools.partial(kernel, n_kv, n_tp, seqs, width), out_sh...]
where the time goes in v6:
time: 76.1 us; the launch traced here: 75.9 us
  Pallas kernels  75.3 us (99%)
    pallas_call x1, Pallas kernels, body(): pl.pallas_call(functools.partial(kernel, n_kv, n_tp, seqs, width), out_sh...  75.3 us

profile of v6, /device:TPU:1, one launch (start us, length us, event | category | flops | bytes accessed | tf_op | source)
XLA Modules:
  0.0 75.9 jit_solution(1645929447422506017)
XLA Ops:
  0.0 75.3 %layer.1 = bf16[16,18]{1,0:T(8,128)(2,1)S(1)} custom-call(bf16[16,18]{1,0:T(8,128)(2,1)} %bitcast.13, f32[6,4096]{1,0:T(8,128)} %gains_h.1, bf16[128,512]{1,0:T(8,128)(2,1)} %wq_h.1, bf16[128,512]{1,0:T(8,128)(2,1)} %wk_h.1, bf16[128,512]{1,0:T(8,128)(2,1)} %wv_h.1, bf16[8,4096]{1,0:T(8,128)(2,1)} %bitcast.12, bf16[44,4096]{1,0:T(8,128)(2,1)} %bitcast.8, ...), custom_call_target="tpu_custom_call" | custom-call | tf_op jit(solution)/shard_map/layer/pallas_call | solution.py:552
  75.3 0.6 copy.18
